TPU v7x, 512 devices: a whole 4x8x8 slice. The times are simulated.
512 devices in a mesh: sp: 64 (over z, y), dp: 8 (over x, core).
Axes of the slice: x: 4, y: 8, z: 8, core: 2. Of those that a mesh axis runs over, the one named last changes fastest.
Arguments:
- tokens: bfloat16 [8192, 2048], P('sp', 'dp'), may hold values from -6 to 6
- cotangent: bfloat16 [8192, 2048], P('sp', 'dp'), may hold values from -6 to 6
- in_weight: bfloat16 [1024, 2048], P('sp', 'dp'), may hold values from -0.125 to 0.125
- out_weight: bfloat16 [1024, 2048], P('sp', 'dp'), may hold values from -0.1875 to 0.1875
- decay_rate: float32 [64, 32], P('sp'), may hold values from 0 to 1
- frequency: float32 [64, 32], P('sp'), may hold values from 4 to 40
- step_log: float32 [64], P('sp'), may hold values from -2.6593 to -1.9661
- drive_real: float32 [64, 32, 16], P('sp'), may hold values from -6 to 6
- drive_imag: float32 [64, 32, 16], P('sp'), may hold values from -6 to 6
- readout_real_part: float32 [64, 16, 32], P('sp'), may hold values from -0.75 to 0.75
- readout_imaginary: float32 [64, 16, 32], P('sp'), may hold values from -0.75 to 0.75
- skip_gain: float32 [64, 16], P('sp'), may hold values from -4 to 4
Outputs:
- grad_tokens: bfloat16 [8192, 2048], P('sp', 'dp')
- grad_in_weight: float32 [1024, 2048], P('sp', 'dp')
- grad_out_weight: float32 [1024, 2048], P('sp', 'dp')
All inputs are finite; a program needn't handle non-finite values.
Results may differ from a plain program's by a relative error of at most 0.02.
Values may be sent and summed in bfloat16 or wider, within the bound.
A program may use at most 64 MiB of HBM per device.

v0:
```python
import jax
import jax.numpy as jnp
from jax import lax
from jax.sharding import PartitionSpec as P

finest_precision = lax.Precision.HIGHEST


def sent_together(arrays, axis, dim, along):
    ends, at = ([], 0)
    for a in arrays[:-1]:
        at += a.shape[along]
        ends.append(at)
    both = jnp.concatenate(arrays, axis=along)
    return tuple(jnp.split(lax.all_gather(both, axis, axis=dim, tiled=True), ends, axis=along))


def split_up(shard, dim, count):
    before, after = (shard.shape[:dim], shard.shape[dim + 1 :])
    return jnp.moveaxis(shard.reshape(*before, count, -1, *after), dim, 0)


def sent_and_summed(shard, axis, dim):
    parts = split_up(shard, dim, lax.axis_size(axis))
    arrived = lax.all_to_all(parts, axis, split_axis=0, concat_axis=0, tiled=True)
    return arrived.astype(jnp.float32).sum(axis=0)


def sent_together_2(arrays, axis, dim, along):
    ends, at = ([], 0)
    for a in arrays[:-1]:
        at += a.shape[along]
        ends.append(at)
    both = jnp.concatenate(arrays, axis=along)
    return tuple(jnp.split(sent_and_summed(both, axis, dim), ends, axis=along))


def in_one_piece(arrays, axis, split_dim, concat_dim, along):
    both = jnp.concatenate(arrays, axis=along)
    out, at, outs = (
        lax.all_to_all(both, axis, split_axis=split_dim, concat_axis=concat_dim, tiled=True),
        0,
        [],
    )
    for a in arrays:
        outs.append(lax.slice_in_dim(out, at, at + a.shape[along], axis=along))
        at += a.shape[along]
    return tuple(outs)


def turned_gather(arrays, axis, dims):
    turned = [jnp.moveaxis(a, dim, 0) for a, dim in zip(arrays, dims)]
    widths = [t[0].size for t in turned]
    both = jnp.concatenate([t.reshape(-1, w) for t, w in zip(turned, widths)], axis=1)
    out = lax.all_gather(both, axis, axis=0, tiled=True)
    parts = jnp.split(out, [sum(widths[:k]) for k in range(1, len(widths))], axis=1)
    return tuple(
        (
            jnp.moveaxis(b.reshape(-1, *t.shape[1:]), 0, dim)
            for b, t, dim in zip(parts, turned, dims)
        )
    )


def summed_on_arrival(shard, axis, dim):
    parts = split_up(shard, dim, lax.axis_size(axis))
    arrived = lax.all_to_all(parts, axis, split_axis=0, concat_axis=0, tiled=True)
    return arrived.sum(axis=0)


def combine(earlier, later):
    first_real, first_imag, first_sum_real, first_sum_imag = earlier
    next_real, next_imag, next_sum_real, next_sum_imag = later
    return (
        first_real * next_real - first_imag * next_imag,
        first_real * next_imag + first_imag * next_real,
        next_real * first_sum_real - next_imag * first_sum_imag + next_sum_real,
        next_real * first_sum_imag + next_imag * first_sum_real + next_sum_imag,
    )


def discretize(decay_rate, frequency, step_log, drive_real, drive_imag):
    step_size = jnp.exp(step_log)[..., None]
    magnitude = jnp.exp(-decay_rate * step_size)
    angle = frequency * step_size
    decay_real = magnitude * jnp.cos(angle)
    decay_imag = magnitude * jnp.sin(angle)
    modulus = decay_rate * decay_rate + frequency * frequency
    hold_real = (-decay_rate * (decay_real - 1.0) + frequency * decay_imag) / modulus
    hold_imag = (-frequency * (decay_real - 1.0) - decay_rate * decay_imag) / modulus
    input_real = hold_real[..., None] * drive_real - hold_imag[..., None] * drive_imag
    input_imag = hold_real[..., None] * drive_imag + hold_imag[..., None] * drive_real
    return (decay_real, decay_imag, input_real, input_imag)


def mechanism(head_drive, head_back, params):
    (
        decay_rate,
        frequency,
        step_log,
        drive_real,
        drive_imag,
        readout_real_part,
        readout_imaginary,
        skip_gain,
    ) = params
    group_count, states = decay_rate.shape
    own_width, length = head_drive.shape
    per_group = own_width // group_count
    block_len = min(512, length)
    blocks_total = length // block_len
    decay_real, decay_imag, input_real, input_imag = discretize(
        decay_rate, frequency, step_log, drive_real, drive_imag
    )
    factor_real = jnp.broadcast_to(decay_real[:, :, None], (group_count, states, block_len))
    factor_imag = jnp.broadcast_to(decay_imag[:, :, None], (group_count, states, block_len))

    def to_blocks(matrix):
        shaped = matrix.astype(jnp.float32).reshape(group_count, per_group, blocks_total, block_len)
        return jnp.moveaxis(shaped, 2, 0)

    def forward(carried, drive_block):
        state_real, state_imag = carried
        push_real = jnp.einsum("gpc,gck->gpk", input_real, drive_block, precision=finest_precision)
        push_imag = jnp.einsum("gpc,gck->gpk", input_imag, drive_block, precision=finest_precision)
        push_real = push_real.at[:, :, 0].add(decay_real * state_real - decay_imag * state_imag)
        push_imag = push_imag.at[:, :, 0].add(decay_real * state_imag + decay_imag * state_real)
        _, _, running_real_part, running_imaginary = lax.associative_scan(
            combine, (factor_real, factor_imag, push_real, push_imag), axis=2
        )
        mixed_rows = (
            jnp.einsum(
                "mow,mwn->mon", readout_real_part, running_real_part, precision=finest_precision
            )
            - jnp.einsum(
                "mow,mwn->mon", readout_imaginary, running_imaginary, precision=finest_precision
            )
            + skip_gain[:, :, None] * drive_block
        )
        return ((running_real_part[:, :, -1], running_imaginary[:, :, -1]), mixed_rows)

    empty_state = jnp.zeros((group_count, states), jnp.float32)
    _, mixed_blocks = lax.scan(forward, (empty_state, empty_state), to_blocks(head_drive))

    def backward(carried, inputs):
        adjoint_real, adjoint_imag = carried
        mixed_rows, back_block = inputs
        gated, pullback = jax.vjp(jax.nn.gelu, mixed_rows)
        (interior_gradient,) = pullback(back_block)
        pulled_real_part = jnp.einsum(
            "woy,wom->wym", readout_real_part, interior_gradient, precision=finest_precision
        )[:, :, ::-1]
        pulled_imaginary = -jnp.einsum(
            "woy,wom->wym", readout_imaginary, interior_gradient, precision=finest_precision
        )[:, :, ::-1]
        pulled_real_part = pulled_real_part.at[:, :, 0].add(
            decay_real * adjoint_real + decay_imag * adjoint_imag
        )
        pulled_imaginary = pulled_imaginary.at[:, :, 0].add(
            decay_real * adjoint_imag - decay_imag * adjoint_real
        )
        _, _, running_real_part, running_imaginary = lax.associative_scan(
            combine, (factor_real, -factor_imag, pulled_real_part, pulled_imaginary), axis=2
        )
        running_real_part = running_real_part[:, :, ::-1]
        running_imaginary = running_imaginary[:, :, ::-1]
        grad_block = (
            jnp.einsum("gpc,gpk->gck", input_real, running_real_part, precision=finest_precision)
            + jnp.einsum("gpc,gpk->gck", input_imag, running_imaginary, precision=finest_precision)
            + skip_gain[:, :, None] * interior_gradient
        )
        return (
            (running_real_part[:, :, 0], running_imaginary[:, :, 0]),
            (grad_block.astype(jnp.bfloat16), gated.astype(jnp.bfloat16)),
        )

    _, (grad_blocks, gated_blocks) = lax.scan(
        backward, (empty_state, empty_state), (mixed_blocks, to_blocks(head_back)), reverse=True
    )

    def from_blocks(stacked):
        return jnp.moveaxis(stacked, 0, 2).reshape(own_width, length)

    return (from_blocks(grad_blocks), from_blocks(gated_blocks))


def on_device(
    tokens,
    cotangent,
    in_weight,
    out_weight,
    decay_rate,
    frequency,
    step_log,
    drive_real,
    drive_imag,
    readout_real_part,
    readout_imaginary,
    skip_gain,
):
    full_in, full_out = sent_together((in_weight, out_weight), "sp", 0, 1)
    part_drive = jnp.einsum(
        "cd,td->ct", full_in, tokens, preferred_element_type=jnp.float32
    ).astype(jnp.bfloat16)
    part_back = jnp.einsum(
        "cd,td->ct", full_out, cotangent, preferred_element_type=jnp.float32
    ).astype(jnp.bfloat16)
    channels = part_drive.shape[0]
    rows_here = tokens.shape[0]
    seq_devices = lax.axis_size("sp")
    own_width = channels // seq_devices
    params = (
        decay_rate,
        frequency,
        step_log,
        drive_real,
        drive_imag,
        readout_real_part,
        readout_imaginary,
        skip_gain,
    )
    row_groups = lax.axis_size("dp")
    portion = rows_here // row_groups
    own_slot = lax.axis_index("dp") * portion
    drive_share, back_share = sent_together_2((part_drive, part_back), "dp", 1, 0)
    drive_slice = drive_share.astype(jnp.bfloat16)[:, None, :]
    back_slice = back_share.astype(jnp.bfloat16)[:, None, :]
    drive_parts, back_parts = in_one_piece((drive_slice, back_slice), "sp", 0, 1, 2)
    drive_joined, back_joined = turned_gather((drive_parts, back_parts), "dp", (2, 2))
    head_grad, head_gated = mechanism(
        drive_joined.reshape(own_width, seq_devices * rows_here),
        back_joined.reshape(own_width, seq_devices * rows_here),
        params,
    )
    grad_slice = lax.dynamic_slice_in_dim(
        head_grad.reshape(own_width, seq_devices, rows_here), own_slot, portion, 2
    )
    gated_slice = lax.dynamic_slice_in_dim(
        head_gated.reshape(own_width, seq_devices, rows_here), own_slot, portion, 2
    )
    grad_parts, gated_parts = in_one_piece((grad_slice, gated_slice), "sp", 1, 0, 2)
    grad_joined, gated_joined = turned_gather((grad_parts, gated_parts), "dp", (2, 2))
    grad_cols = grad_joined.reshape(channels, rows_here)
    gated_cols = gated_joined.reshape(channels, rows_here)
    grad_tokens = jnp.einsum(
        "ct,cd->td", grad_cols, full_in, preferred_element_type=jnp.float32
    ).astype(jnp.bfloat16)
    grad_scale = (rows_here * seq_devices) ** (-0.5)
    picked = grad_cols
    grad_in_weight = summed_on_arrival(
        jnp.einsum("ct,td->cd", picked, tokens, preferred_element_type=jnp.float32) * grad_scale,
        "sp",
        0,
    )
    picked = gated_cols
    grad_out_weight = summed_on_arrival(
        jnp.einsum("ct,td->cd", picked, cotangent, preferred_element_type=jnp.float32) * grad_scale,
        "sp",
        0,
    )
    return (grad_tokens, grad_in_weight, grad_out_weight)


def solution(mesh):
    return jax.shard_map(
        on_device,
        mesh=mesh,
        in_specs=(
            P("sp", "dp"),
            P("sp", "dp"),
            P("sp", "dp"),
            P("sp", "dp"),
            P("sp", None),
            P("sp", None),
            P("sp"),
            P("sp", None, None),
            P("sp", None, None),
            P("sp", None, None),
            P("sp", None, None),
            P("sp", None),
        ),
        out_specs=(P("sp", "dp"), P("sp", "dp"), P("sp", "dp")),
        check_vma=False,
    )
```

profile of v0, /device:TPU:1, one launch (start us, length us, event | category | flops | bytes accessed | tf_op | source)
XLA Modules:
  0.0 1625.2 jit_solution(3426954603965200112)
XLA Ops:
  7.2 1.4 pad_maximum_fusion.37
  10.0 84.4 %all-gather.2.cloned.1.call-done = bf16[1024,512]{1,0:T(8,128)(2,1)} async-done(((bf16[16,512]{1,0:T(8,128)(2,1)}), bf16[1024,512]{1,0:T(8,128)(2,1)}) %all-gather.2.cloned.1.call-update) | async-done | bytes 1048592 | tf_op jit(solution)/shard_map/all_gather | solution.py:15
  94.5 1.3 convolution_convert_fusion
  95.8 1.3 convolution_convert_fusion.1
  98.2 9.8 all-to-all-start
  109.7 7.6 all-to-all-done
  119.6 8.6 all-to-all-start.1
  128.2 11.1 all-to-all-done.1
  140.7 15.3 all_gather.10
  158.4 657.2 %while.40 = (s32[]{:T(128)}, f32[1,32]{1,0:T(1,128)S(1)}, f32[1,32]{1,0:T(1,128)S(1)}, f32[16,1,16,512]{3,2,1,0:T(8,128)S(1)}, f32[16,1,16,512]{3,0,2,1:T(8,128)...) while((s32[]{:T(128)}, f32[1,32]{1,0:T(1,128)S(1)}, ...), condition=%wide.region_2.0_spmd, body=%wide.region_1.2_spmd.sunk | while | flops 12997378 | bytes 4572589 | solution.py:143
  162.9 1.1 slice.2949
  203.9 1.1 slice.2949
  245.0 1.1 slice.2949
  286.0 1.1 slice.2949
  327.1 1.1 slice.2949
  368.2 1.1 slice.2949
  409.2 1.1 slice.2949
  450.3 1.1 slice.2949
  491.4 1.1 slice.2949
  532.4 1.1 slice.2949
  573.5 1.1 slice.2949
  614.5 1.1 slice.2949
  655.6 1.1 slice.2949
  696.7 1.1 slice.2949
  737.7 1.1 slice.2949
  778.8 1.1 slice.2949
  817.1 699.5 %while.41 = (s32[]{:T(128)}, f32[1,32]{1,0:T(1,128)S(1)}, f32[1,32]{1,0:T(1,128)S(1)}, bf16[16,1,16,512]{3,2,1,0:T(8,128)(2,1)S(1)}, bf16[16,1,16,512]{3,2,1,0:T...) while((s32[]{:T(128)}, f32[1,32]{1,0:T(1,128)S(1)}, ...), condition=%wide.region_4.5_spmd, body=%wide.region_3.0_spmd.sunk | while | flops 13562627 | bytes 5699549 | solution.py:177
  838.8 1.1 slice.3074
  872.9 1.1 pad.1037
  881.4 1.1 slice.3074
  915.6 1.1 pad.1037
  924.1 1.1 slice.3074
  958.2 1.1 pad.1037
  966.8 1.1 slice.3074
  1000.9 1.1 pad.1037
  1009.4 1.1 slice.3074
  1043.6 1.1 pad.1037
  1052.1 1.1 slice.3074
  1086.2 1.1 pad.1037
  1094.8 1.1 slice.3074
  1128.9 1.1 pad.1037
  1137.4 1.1 slice.3074
  1171.6 1.1 pad.1037
  1214.2 1.1 pad.1037
  1222.8 1.1 slice.3074
  1256.9 1.1 pad.1037
  1265.4 1.1 slice.3074
  1299.6 1.1 pad.1037
  1342.2 1.1 pad.1037
  1384.9 1.1 pad.1037
  1393.4 1.1 slice.3074
  1427.6 1.1 pad.1037
  1470.2 1.1 pad.1037
  1478.8 1.1 slice.3074
  1512.9 1.1 pad.1037
  1518.0 14.9 all_to_all.51
  1533.5 14.3 all_gather.11
  1547.8 1.3 convolution_multiply_fusion.1
  1549.1 4.7 all-to-all-start.3
  1553.7 1.3 convolution_multiply_fusion
  1555.0 27.2 %all-to-all-done.3 = f32[64,16,256]{2,1,0:T(8,128)S(1)} async-done(((f32[64,16,256]{2,1,0:T(8,128)}), f32[64,16,256]{2,1,0:T(8,128)S(1)}, u32[]{:S(2)}, u32[]{:S(2)}) %all-to-all-start.3) | async-done | bytes 1048608 | tf_op jit(solution)/shard_map/all_to_all | solution.py:67
  1582.2 8.1 all-to-all-start.4
  1590.3 1.9 convolution_convert_fusion.2
  1592.9 24.5 %all-to-all-done.4 = f32[64,16,256]{2,1,0:T(8,128)S(1)} async-done(((f32[64,16,256]{2,1,0:T(8,128)}), f32[64,16,256]{2,1,0:T(8,128)S(1)}, u32[]{:S(2)}, u32[]{:S(2)}) %all-to-all-start.4) | async-done | bytes 1048608 | tf_op jit(solution)/shard_map/all_to_all | solution.py:67
  (5664 shorter events, 1273.5 us)
Async XLA Ops:
  7.2 88.6 %copy-start = (bf16[128,256]{1,0:T(8,128)(2,1)S(1)}, bf16[128,256]{1,0:T(8,128)(2,1)}, u32[]{:S(2)}) copy-start(bf16[128,256]{1,0:T(8,128)(2,1)} %param.24) | copy-start | bytes 196612
  7.2 87.3 %copy-start.1 = (bf16[128,256]{1,0:T(8,128)(2,1)S(1)}, bf16[128,256]{1,0:T(8,128)(2,1)}, u32[]{:S(2)}) copy-start(bf16[128,256]{1,0:T(8,128)(2,1)} %param.25) | copy-start | bytes 196612
  7.2 87.3 %all-gather.2.cloned.1.call-start = ((), (), s32[]{:S(2)}) async-start(), calls=%async_computation.5 | async-start | bytes 1064960 | tf_op jit(solution)/shard_map/all_gather | solution.py:15
  98.2 19.1 %all-to-all-start = ((bf16[8,2048,16]{1,2,0:T(8,128)(2,1)}), bf16[8,2048,16]{1,2,0:T(8,128)(2,1)S(1)}, u32[]{:S(2)}, u32[]{:S(2)}) async-start(bf16[8,2048,16]{1,2,0:T(8,128)(2,1)} %bitcast.37), calls=%async_computation | async-start | bytes 1048576 | tf_op jit(solution)/shard_map/all_to_all | solution.py:25
  108.0 0.7 copy-start.7
  108.0 0.7 copy-start.8
  108.7 0.7 copy-start.6
  108.8 0.7 copy-start.5
  119.6 19.7 %all-to-all-start.1 = ((bf16[64,2,256]{2,1,0:T(2,128)(2,1)}), bf16[64,2,256]{2,1,0:T(2,128)(2,1)S(1)}, u32[]{:S(2)}, u32[]{:S(2)}) async-start(bf16[64,2,256]{2,1,0:T(2,128)(2,1)} %reshape.636), calls=%async_computation.1 | async-start | bytes 131072 | tf_op jit(solution)/shard_map/all_to_all | solution.py:41
  157.6 0.7 copy-start.2
  157.6 0.7 copy-start.3
  157.7 0.7 copy-start.4
  1549.1 33.1 %all-to-all-start.3 = ((f32[64,16,256]{2,1,0:T(8,128)}), f32[64,16,256]{2,1,0:T(8,128)S(1)}, u32[]{:S(2)}, u32[]{:S(2)}) async-start(f32[64,16,256]{2,1,0:T(8,128)} %bitcast.72), calls=%async_computation.3 | async-start | bytes 2097152 | tf_op jit(solution)/shard_map/all_to_all | solution.py:67
  1582.2 35.2 %all-to-all-start.4 = ((f32[64,16,256]{2,1,0:T(8,128)}), f32[64,16,256]{2,1,0:T(8,128)S(1)}, u32[]{:S(2)}, u32[]{:S(2)}) async-start(f32[64,16,256]{2,1,0:T(8,128)} %bitcast.76), calls=%async_computation.4 | async-start | bytes 2097152 | tf_op jit(solution)/shard_map/all_to_all | solution.py:67
Sparse Core Ops, SparseCore 0:
  11.6 82.7 all-gather.1
where the time goes:
time: 1630 us
  local copies, waits for them, and re-layouts  1220 us (75%)
  waiting for transfers between devices  155 us (10%)
  other arithmetic  76.4 us (5%)
  loops' own time  47.2 us (3%)
  blocking collectives  44.5 us (3%)
  matrix products  32.6 us (2%)
  starting transfers between devices  31.2 us (2%)
    slice x1264, local copies, waits for them, and re-layouts, forward(): lax.associative_scan(combine, (factor_real, factor_imag, push_real, push_...  423 us
    slice x1263, local copies, waits for them, and re-layouts, backward(): lax.associative_scan(combine, (factor_real, -factor_imag, pulled_real_par...  422 us
    pad x512, local copies, waits for them, and re-layouts, backward(): lax.associative_scan(combine, (factor_real, -factor_imag, pulled_real_par...  167 us
    pad x512, local copies, waits for them, and re-layouts, forward(): lax.associative_scan(combine, (factor_real, factor_imag, push_real, push_...  167 us
    all_gather x1, waiting for transfers between devices, sent_together(): lax.all_gather(both, axis, axis=dim, tiled=True)  84.4 us
    all_to_all x2, waiting for transfers between devices, summed_on_arrival(): lax.all_to_all(parts, axis, split_axis=0, concat_axis=0, tiled=True)  51.7 us

commit v1 on v0

v1 whole, which is shorter than its diff:
```python
import functools
import math

import jax
import jax.numpy as jnp
from jax import lax
from jax.experimental import pallas as pl
from jax.experimental.pallas import tpu as pltpu
from jax.sharding import PartitionSpec as P

MESH = pl.DeviceIdType.MESH
F32 = jnp.float32
BF16 = jnp.bfloat16
HIGHEST = lax.Precision.HIGHEST

(
    IN_A1, IN_B1, IN_A2, IN_B2, OUT_A1, OUT_B1, OUT_A2, OUT_B2,
    PK_Z, AUX_Z, PK_Y, AUX_Y, DRIVE, BACK, FWD_Y, FWD_Z, BWD_Y, BWD_Z,
    GATED, MIX, GO_A1, GO_B1, GO_A2, GO_B2, GI_A1, GI_B1, GI_A2, GI_B2,
) = range(28)
PHASES = 28

NN = (((1,), (0,)), ((), ()))
NT = (((1,), (1,)), ((), ()))
TN = (((0,), (0,)), ((), ()))


def dot(a, b, dims=NN, precision=None):
    return lax.dot_general(a, b, dims, precision=precision, preferred_element_type=F32)


def cmul(a, b):
    return a[0] * b[0] - a[1] * b[1], a[0] * b[1] + a[1] * b[0]


def conj(a):
    return a[0], -a[1]


def square(a, times):
    for _ in range(times):
        a = (a[0] * a[0] - a[1] * a[1], 2.0 * a[0] * a[1])
    return a


def log2(n):
    return n.bit_length() - 1


def iota(shape, dim):
    return lax.broadcasted_iota(jnp.int32, shape, dim)


def scan_rows(pair, decay, reverse):
    re, im = pair
    rows, lanes = re.shape
    width = min(128, lanes)
    row = iota((rows, width), 0)
    outs = []
    for at in range(0, lanes, width):
        a, b = re[:, at : at + width], im[:, at : at + width]
        f = (decay[0][:, at : at + width], decay[1][:, at : at + width])
        for k in range(log2(rows)):
            step = 1 << k
            if reverse:
                turn, keep = rows - step, row < rows - step
            else:
                turn, keep = step, row >= step
            ra = jnp.where(keep, pltpu.roll(a, turn, 0), 0.0)
            rb = jnp.where(keep, pltpu.roll(b, turn, 0), 0.0)
            a, b = a + f[0] * ra - f[1] * rb, b + f[0] * rb + f[1] * ra
            f = square(f, 1)
        outs.append((a, b))
    return (
        jnp.concatenate([o[0] for o in outs], axis=1),
        jnp.concatenate([o[1] for o in outs], axis=1),
    )


def kernel(
    ny, nz, nd,
    tok, cot, win, wout, rate, freq, slog, dr, di, rr, ri, skip,
    o_tok, o_in, o_out,
    pk_own, aux_own, pk_z, aux_z, pk_y, aux_y,
    wa_in, wb_in, wa_out, wb_out,
    d_send, d_recv, b_send, b_recv,
    f_own, f_recv, t_own, t_recv, a_own, a_recv, q_own, q_recv,
    gat_own, gat_all, mix_own, mix_all,
    go_sa, go_sb, go_ra, go_rb, go_s2a, go_s2b, go_r2a, go_r2b,
    gi_sa, gi_sb, gi_ra, gi_rb, gi_s2a, gi_s2b, gi_r2a, gi_r2b,
    bre, bim, cre, cim, u_re, u_im, v_re, v_im,
    ssem, rsem,
):
    sp, dp = lax.axis_index("sp"), lax.axis_index("dp")
    z, y = lax.div(sp, ny), lax.rem(sp, ny)
    size = {"y": ny, "z": nz, "d": nd}
    here = {"y": y, "z": z, "d": dp}
    rows = tok.shape[0]
    states = rate.shape[1]
    per_group = skip.shape[1]
    own_ch = ny * per_group
    lanes = ny * states
    half = win.shape[1] // 2

    def device(axis, j):
        if axis == "y":
            return (z * ny + j, dp)
        if axis == "z":
            return (j * ny + y, dp)
        return (sp, j)

    def copy(phase, axis, k, src, dst):
        j = lax.rem(here[axis] + k, size[axis])
        return pltpu.make_async_remote_copy(
            src_ref=src(j),
            dst_ref=dst,
            send_sem=ssem.at[phase, k],
            recv_sem=rsem.at[phase, k],
            device_id=device(axis, j),
            device_id_type=MESH,
        )

    sent = []

    def send(phase, axis, src, dst):
        for k in range(1, size[axis]):
            copy(phase, axis, k, src, dst).start()
        sent.append((phase, axis, src, dst))

    def arrive(phase, axis, slot):
        n = size[axis]
        for k in range(1, n):
            j = lax.rem(here[axis] + (n - k), n)
            copy(phase, axis, k, lambda _: slot(j), slot(j)).wait_recv()

    barrier = pltpu.get_barrier_semaphore()
    for axis in ("y", "z", "d"):
        for k in range(1, size[axis]):
            j = lax.rem(here[axis] + k, size[axis])
            pl.semaphore_signal(barrier, inc=1, device_id=device(axis, j), device_id_type=MESH)

    tile_s = (iota((states, lanes), 0) == lax.rem(iota((states, lanes), 1), states)).astype(F32)
    wide = lambda ref: dot(jnp.broadcast_to(ref[...], (8, states)), tile_s, precision=HIGHEST)
    rate_w, freq_w = wide(rate), wide(freq)
    step = jnp.exp(jnp.full((8, lanes), slog[0], F32))
    magnitude = jnp.exp(-rate_w * step)
    angle = freq_w * step
    dec_re, dec_im = magnitude * jnp.cos(angle), magnitude * jnp.sin(angle)
    modulus = rate_w * rate_w + freq_w * freq_w
    hold_re = (-rate_w * (dec_re - 1.0) + freq_w * dec_im) / modulus
    hold_im = (-freq_w * (dec_re - 1.0) - rate_w * dec_im) / modulus
    tile_c = (
        iota((per_group, lanes), 0) == lax.rem(iota((per_group, lanes), 1), per_group)
    ).astype(F32)
    skip_w = dot(jnp.broadcast_to(skip[...], (8, per_group)), tile_c, precision=HIGHEST)
    row8 = iota((8, lanes), 0)
    aux_own[...] = jnp.where(row8 == 0, dec_re, jnp.where(row8 == 1, dec_im, skip_w))
    four = 4 * states
    p_row, p_lane = iota((states, four), 0), iota((states, four), 1)
    hr, hi = hold_re[0:1, 0:states], hold_im[0:1, 0:states]
    hr = jnp.concatenate([hr] * 4, axis=1) if four > lanes else hold_re[0:1, 0:four]
    hi = jnp.concatenate([hi] * 4, axis=1) if four > lanes else hold_im[0:1, 0:four]
    first, second = p_lane == p_row, p_lane == p_row + states
    sel_r = jnp.where(first, hr, 0.0) + jnp.where(second, hi, 0.0)
    sel_i = jnp.where(first, -hi, 0.0) + jnp.where(second, hr, 0.0)
    sel_c = (p_lane == p_row + 2 * states).astype(F32)
    sel_d = (p_lane == p_row + 3 * states).astype(F32)
    pk_own[...] = (
        dot(dr[0], sel_r, NN, HIGHEST)
        + dot(di[0], sel_i, NN, HIGHEST)
        + dot(rr[0], sel_c, NN, HIGHEST)
        + dot(ri[0], sel_d, NN, HIGHEST)
    ).astype(BF16)

    pl.semaphore_wait(barrier, (ny - 1) + (nz - 1) + (nd - 1))

    send(IN_A1, "y", lambda j: win.at[:, 0:half], wa_in.at[z, y])
    send(IN_B1, "z", lambda j: win.at[:, half:], wb_in.at[y, z])

    def param_copy(phase, k, src, dst):
        j = lax.rem(z + k, nz)
        return pltpu.make_async_remote_copy(
            src_ref=src, dst_ref=dst, send_sem=ssem.at[phase, k], recv_sem=rsem.at[phase, 0],
            device_id=(j * ny + y, dp), device_id_type=MESH,
        )

    @pl.when(z == dp)
    def _():
        for k in range(1, nz):
            param_copy(PK_Z, k, pk_own, pk_z).start()
            param_copy(AUX_Z, k, aux_own, aux_z).start()
        pk_z[...] = pk_own[...]
        aux_z[...] = aux_own[...]

    send(OUT_A1, "y", lambda j: wout.at[:, 0:half], wa_out.at[z, y])
    send(OUT_B1, "z", lambda j: wout.at[:, half:], wb_out.at[y, z])
    wa_in[z, y] = win[:, 0:half]
    wb_in[y, z] = win[:, half:]
    wa_out[z, y] = wout[:, 0:half]
    wb_out[y, z] = wout[:, half:]

    arrive(IN_A1, "y", lambda j: wa_in.at[z, j])
    send(IN_A2, "z", lambda j: wa_in.at[z], wa_in.at[z])
    arrive(IN_B1, "z", lambda j: wb_in.at[y, j])
    send(IN_B2, "y", lambda j: wb_in.at[y], wb_in.at[y])

    @pl.when(z != dp)
    def _():
        param_copy(PK_Z, 1, pk_z, pk_z).wait_recv()
        param_copy(AUX_Z, 1, aux_z, aux_z).wait_recv()

    send(PK_Y, "y", lambda j: pk_z, pk_y.at[y])
    send(AUX_Y, "y", lambda j: aux_z, aux_y.at[y])
    pk_y[y] = pk_z[...]
    aux_y[y] = aux_z[...]

    arrive(OUT_A1, "y", lambda j: wa_out.at[z, j])
    send(OUT_A2, "z", lambda j: wa_out.at[z], wa_out.at[z])
    arrive(OUT_B1, "z", lambda j: wb_out.at[y, j])
    send(OUT_B2, "y", lambda j: wb_out.at[y], wb_out.at[y])

    arrive(PK_Y, "y", lambda j: pk_y.at[j])
    arrive(AUX_Y, "y", lambda j: aux_y.at[j])
    packed = pk_y[...].reshape(own_ch, four)
    diag = lax.div(iota((own_ch, lanes), 0), per_group) == lax.div(iota((own_ch, lanes), 1), states)
    s_row, s_lane = iota((four, lanes), 0), lax.rem(iota((four, lanes), 1), states)
    for at, ref in enumerate((bre, bim, cre, cim)):
        spread = (s_row == s_lane + at * states).astype(F32).astype(BF16)
        ref[...] = jnp.where(diag, dot(packed, spread), 0.0).astype(BF16)
    group_of_lane = lax.div(iota((1, lanes), 1), states)
    group_of_ch = lax.div(iota((1, own_ch), 1), per_group)
    dec = (jnp.zeros((1, lanes), F32), jnp.zeros((1, lanes), F32))
    gain = jnp.zeros((1, own_ch), F32)
    for g in range(ny):
        dec = (
            jnp.where(group_of_lane == g, aux_y[g, 0:1, :], dec[0]),
            jnp.where(group_of_lane == g, aux_y[g, 1:2, :], dec[1]),
        )
        gain = jnp.where(group_of_ch == g, aux_y[g, 2:3, 0:own_ch], gain)
    row = iota((rows, lanes), 0)
    up = (jnp.ones((rows, lanes), F32), jnp.zeros((rows, lanes), F32))
    down = up
    factor = dec
    for k in range(log2(rows)):
        bit = lax.rem(lax.div(row, 1 << k), 2) == 1
        more = cmul(up, factor)
        up = (jnp.where(bit, more[0], up[0]), jnp.where(bit, more[1], up[1]))
        more = cmul(down, factor)
        down = (jnp.where(bit, down[0], more[0]), jnp.where(bit, down[1], more[1]))
        factor = square(factor, 1)
    u_re[...], u_im[...] = up
    v_re[...], v_im[...] = down
    dec_chunk = factor
    dec_row = square(dec_chunk, log2(ny))

    def weights_of(wa, wb, b):
        left = wa[b].reshape(own_ch, half)
        right = wb[:, b].reshape(own_ch, half)
        return jnp.concatenate([left, right], axis=1)

    def gathered(phase_a, phase_b, wa, wb):
        arrive(phase_a, "z", lambda j: wa.at[j])
        arrive(phase_b, "y", lambda j: wb.at[j])

    def project(act, wa, wb, out):
        for b in range(nd):
            out[b] = dot(act[...], weights_of(wa, wb, b), NT).astype(BF16)

    def total(recv):
        s = recv[0].astype(F32)
        for b in range(1, nd):
            s = s + recv[b].astype(F32)
        return s.astype(BF16)

    gathered(IN_A2, IN_B2, wa_in, wb_in)
    project(tok, wa_in, wb_in, d_send)
    send(DRIVE, "d", lambda j: d_send.at[j], d_recv.at[dp])
    d_recv[dp] = d_send[dp]
    arrive(DRIVE, "d", lambda j: d_recv.at[j])
    x = total(d_recv)

    def carried(recv, n, me, decay, reverse):
        zero = jnp.zeros((1, lanes), F32)
        enter, whole, power = (zero, zero), (zero, zero), (zero + 1.0, zero)
        for i in range(n):
            j = n - 1 - i if reverse else i
            piece = (recv[j, 0:1, :], recv[j, 1:2, :])
            before = j > me if reverse else j < me
            grown = cmul(enter, decay)
            enter = (
                jnp.where(before, grown[0] + piece[0], enter[0]),
                jnp.where(before, grown[1] + piece[1], enter[1]),
            )
            grown = cmul(whole, decay)
            whole = (grown[0] + piece[0], grown[1] + piece[1])
            grown = cmul(power, decay)
            power = (
                jnp.where(before, grown[0], power[0]),
                jnp.where(before, grown[1], power[1]),
            )
        return enter, whole, power

    def summed(pair, table_re, table_im, sign):
        tr, ti = table_re[...], sign * table_im[...]
        re, im = cmul(pair, (tr, ti))
        return jnp.sum(re, axis=0, keepdims=True), jnp.sum(im, axis=0, keepdims=True)

    def put(ref, pair):
        ref[0:1, :] = pair[0]
        ref[1:2, :] = pair[1]

    push = (dot(x, bre[...]), dot(x, bim[...]))
    final = summed(push, v_re, v_im, 1.0)
    put(f_own, final)
    send(FWD_Y, "y", lambda j: f_own, f_recv.at[y])
    put(f_recv.at[y], final)
    local = scan_rows(push, dec, False)
    arrive(FWD_Y, "y", lambda j: f_recv.at[j])
    enter_y, whole_y, power_y = carried(f_recv, ny, y, dec_chunk, False)
    put(t_own, whole_y)
    send(FWD_Z, "z", lambda j: t_own, t_recv.at[z])
    put(t_recv.at[z], whole_y)

    gathered(OUT_A2, OUT_B2, wa_out, wb_out)
    project(cot, wa_out, wb_out, b_send)
    send(BACK, "d", lambda j: b_send.at[j], b_recv.at[dp])
    b_recv[dp] = b_send[dp]

    arrive(FWD_Z, "z", lambda j: t_recv.at[j])
    enter_z, _, _ = carried(t_recv, nz, z, dec_row, False)
    far = cmul(power_y, enter_z)
    start = cmul(dec, (enter_y[0] + far[0], enter_y[1] + far[1]))
    add = cmul((u_re[...], u_im[...]), start)
    state_re, state_im = (local[0] + add[0]).astype(BF16), (local[1] + add[1]).astype(BF16)
    mixed = dot(state_re, cre[...], NT) - dot(state_im, cim[...], NT) + gain * x.astype(F32)
    c0 = math.sqrt(2.0 / math.pi)
    sq = mixed * mixed
    th = jnp.tanh(c0 * mixed * (1.0 + 0.044715 * sq))
    half_up = 0.5 * (1.0 + th)
    gated = (mixed * half_up).astype(BF16)
    slope = half_up + 0.5 * mixed * (1.0 - th * th) * (c0 * (1.0 + 3.0 * 0.044715 * sq))
    gat_own[...] = gated
    send(GATED, "d", lambda j: gat_own, gat_all.at[dp])
    gat_all[dp] = gated

    arrive(BACK, "d", lambda j: b_recv.at[j])
    inner = slope * total(b_recv).astype(F32)
    inner_b = inner.astype(BF16)
    pulled = (dot(inner_b, cre[...]), -dot(inner_b, cim[...]))
    opening = summed(pulled, u_re, u_im, -1.0)
    put(a_own, opening)
    send(BWD_Y, "y", lambda j: a_own, a_recv.at[y])
    put(a_recv.at[y], opening)
    back_dec = conj(dec)
    local = scan_rows(pulled, back_dec, True)
    arrive(BWD_Y, "y", lambda j: a_recv.at[j])
    enter_y, whole_y, power_y = carried(a_recv, ny, y, conj(dec_chunk), True)
    put(q_own, whole_y)
    send(BWD_Z, "z", lambda j: q_own, q_recv.at[z])
    put(q_recv.at[z], whole_y)

    def weight_grad(phase_a, phase_b, cols, act, sa, sb, ra, rb):
        for b in range(nd):
            part = dot(cols[b], act[...], TN).astype(BF16)
            sa[b] = part[:, 0:half].reshape(ny, per_group, half)
            sb[:, b] = part[:, half:].reshape(ny, per_group, half)
        send(phase_a, "z", lambda j: sa.at[j], ra.at[z])
        send(phase_b, "y", lambda j: sb.at[j], rb.at[y])
        ra[z] = sa[z]
        rb[y] = sb[y]

    def reduced(recv, n):
        s = recv[0].astype(F32)
        for j in range(1, n):
            s = s + recv[j].astype(F32)
        return s

    def second_step(phase_a1, phase_b1, phase_a2, phase_b2, ra, rb, s2a, s2b, r2a, r2b):
        arrive(phase_a1, "z", lambda j: ra.at[j])
        s2a[...] = reduced(ra, nz).astype(BF16)
        send(phase_a2, "y", lambda j: s2a.at[j], r2a.at[y])
        r2a[y] = s2a[y]
        arrive(phase_b1, "y", lambda j: rb.at[j])
        s2b[...] = reduced(rb, ny).astype(BF16)
        send(phase_b2, "z", lambda j: s2b.at[j], r2b.at[z])
        r2b[z] = s2b[z]

    scale = (rows * ny * nz) ** -0.5

    def finish(phase_a2, phase_b2, r2a, r2b, out):
        arrive(phase_a2, "y", lambda j: r2a.at[j])
        arrive(phase_b2, "z", lambda j: r2b.at[j])
        out[:, 0:half] = reduced(r2a, ny) * scale
        out[:, half:] = reduced(r2b, nz) * scale

    arrive(GATED, "d", lambda j: gat_all.at[j])
    weight_grad(GO_A1, GO_B1, gat_all, cot, go_sa, go_sb, go_ra, go_rb)

    arrive(BWD_Z, "z", lambda j: q_recv.at[j])
    enter_z, _, _ = carried(q_recv, nz, z, conj(dec_row), True)
    far = cmul(power_y, enter_z)
    start = cmul(back_dec, (enter_y[0] + far[0], enter_y[1] + far[1]))
    add = cmul((v_re[...], -v_im[...]), start)
    adj_re, adj_im = (local[0] + add[0]).astype(BF16), (local[1] + add[1]).astype(BF16)
    mix = (dot(adj_re, bre[...], NT) + dot(adj_im, bim[...], NT) + gain * inner).astype(BF16)
    mix_own[...] = mix
    send(MIX, "d", lambda j: mix_own, mix_all.at[dp])
    mix_all[dp] = mix

    second_step(GO_A1, GO_B1, GO_A2, GO_B2, go_ra, go_rb, go_s2a, go_s2b, go_r2a, go_r2b)
    arrive(MIX, "d", lambda j: mix_all.at[j])
    weight_grad(GI_A1, GI_B1, mix_all, tok, gi_sa, gi_sb, gi_ra, gi_rb)
    grad = dot(mix_all[0], weights_of(wa_in, wb_in, 0))
    for b in range(1, nd):
        grad = grad + dot(mix_all[b], weights_of(wa_in, wb_in, b))
    o_tok[...] = grad.astype(BF16)
    finish(GO_A2, GO_B2, go_r2a, go_r2b, o_out)
    second_step(GI_A1, GI_B1, GI_A2, GI_B2, gi_ra, gi_rb, gi_s2a, gi_s2b, gi_r2a, gi_r2b)
    finish(GI_A2, GI_B2, gi_r2a, gi_r2b, o_in)

    @pl.when(z == dp)
    def _():
        for k in range(1, nz):
            param_copy(PK_Z, k, pk_own, pk_z).wait_send()
            param_copy(AUX_Z, k, aux_own, aux_z).wait_send()

    for phase, axis, src, dst in sent:
        for k in range(1, size[axis]):
            copy(phase, axis, k, src, dst).wait_send()


def on_device(ny, nz, nd, tok, cot, win, wout, rate, freq, slog, dr, di, rr, ri, skip):
    rows, cols = tok.shape
    half = cols // 2
    states, c = rate.shape[1], skip.shape[1]
    own_ch, lanes, four = ny * c, ny * states, 4 * states
    V = pltpu.VMEM
    grads = [
        V((nz, ny, c, half), BF16), V((ny, nz, c, half), BF16),
        V((nz, ny, c, half), BF16), V((ny, nz, c, half), BF16),
        V((ny, c, half), BF16), V((nz, c, half), BF16),
        V((ny, c, half), BF16), V((nz, c, half), BF16),
    ]
    most = max(ny, nz, nd)
    vm = pl.BlockSpec(memory_space=pltpu.VMEM)
    return pl.pallas_call(
        functools.partial(kernel, ny, nz, nd),
        out_shape=(
            jax.ShapeDtypeStruct((rows, cols), BF16),
            jax.ShapeDtypeStruct(win.shape, F32),
            jax.ShapeDtypeStruct(wout.shape, F32),
        ),
        in_specs=[vm] * 6 + [pl.BlockSpec(memory_space=pltpu.SMEM)] + [vm] * 5,
        out_specs=(vm, vm, vm),
        scratch_shapes=[
            V((c, four), BF16), V((8, lanes), F32),
            V((c, four), BF16), V((8, lanes), F32),
            V((ny, c, four), BF16), V((ny, 8, lanes), F32),
            V((nz, ny, c, half), BF16), V((ny, nz, c, half), BF16),
            V((nz, ny, c, half), BF16), V((ny, nz, c, half), BF16),
            V((nd, rows, own_ch), BF16), V((nd, rows, own_ch), BF16),
            V((nd, rows, own_ch), BF16), V((nd, rows, own_ch), BF16),
            V((2, lanes), F32), V((ny, 2, lanes), F32),
            V((2, lanes), F32), V((nz, 2, lanes), F32),
            V((2, lanes), F32), V((ny, 2, lanes), F32),
            V((2, lanes), F32), V((nz, 2, lanes), F32),
            V((rows, own_ch), BF16), V((nd, rows, own_ch), BF16),
            V((rows, own_ch), BF16), V((nd, rows, own_ch), BF16),
            *grads, *grads,
            *[V((own_ch, lanes), BF16)] * 4,
            *[V((rows, lanes), F32)] * 4,
            pltpu.SemaphoreType.DMA((PHASES, most)),
            pltpu.SemaphoreType.DMA((PHASES, most)),
        ],
        compiler_params=pltpu.CompilerParams(
            collective_id=0, has_side_effects=True, vmem_limit_bytes=48 * 1024 * 1024
        ),
        name="mixer",
    )(tok, cot, win, wout, rate, freq, slog, jnp.swapaxes(dr, 1, 2), jnp.swapaxes(di, 1, 2), rr, ri, skip)


def solution(mesh):
    nd = mesh.shape["dp"]
    nz = nd
    ny = mesh.shape["sp"] // nz
    return jax.shard_map(
        functools.partial(on_device, ny, nz, nd),
        mesh=mesh,
        in_specs=(
            P("sp", "dp"), P("sp", "dp"), P("sp", "dp"), P("sp", "dp"),
            P("sp", None), P("sp", None), P("sp"),
            P("sp", None, None), P("sp", None, None), P("sp", None, None), P("sp", None, None),
            P("sp", None),
        ),
        out_specs=(P("sp", "dp"), P("sp", "dp"), P("sp", "dp")),
        check_vma=False,
    )
```

time: 1630 us -> 90.6 us (0.06)
  local copies, waits for them, and re-layouts: 1220 us -> 8.36 us
  waiting for transfers between devices: 155 us -> 0 us
  Pallas kernels: 0 us -> 80.4 us
  other arithmetic: 76.4 us -> 0 us
  loops' own time: 47.2 us -> 0 us
  blocking collectives: 44.5 us -> 0 us
  matrix products: 32.6 us -> 0 us
  starting transfers between devices: 31.2 us -> 0 us
    slice x2527 -> x0, local copies, waits for them, and re-layouts: 845 us -> none  [the longest x1264 423 us: forward(): lax.associative_scan(combine, (factor_real, factor_imag, push_real, push_...]
    pad x1024 -> x0, local copies, waits for them, and re-layouts: 335 us -> none  [the longest x512 167 us: backward(): lax.associative_scan(combine, (factor_real, -factor_imag, pulled_real_par...]
    all_gather x1 -> x0, waiting for transfers between devices: 84.4 us -> none  [sent_together(): lax.all_gather(both, axis, axis=dim, tiled=True)]
    pallas_call x0 -> x1, Pallas kernels: none -> 80.4 us  [on_device(): pl.pallas_call(functools.partial(kernel, ny, nz, nd), out_shape=(jax.Shap...]
    all_to_all x4 -> x0, waiting for transfers between devices: 70.3 us -> none  [the longest x2 51.7 us: summed_on_arrival(): lax.all_to_all(parts, axis, split_axis=0, concat_axis=0, tiled=True)]
    another operation x2 -> x0, loops' own time: 47.2 us -> none  [the longest x1 32.2 us: mechanism(): lax.scan(backward, (empty_state, empty_state), (mixed_blocks, to_blocks(h...]
    concatenate x503 -> x0, other arithmetic: 40.2 us -> none  [the longest x256 19.6 us: backward(): lax.associative_scan(combine, (factor_real, -factor_imag, pulled_real_par...]
    dot_general x133 -> x0, matrix products: 32.6 us -> none  [the longest x16 4.03 us: backward(): jnp.einsum('woy,wom->wym', readout_real_part, interior_gradient, precisio...]
where the time goes in v1:
time: 90.6 us; the launch traced here: 90.1 us
  Pallas kernels  80.4 us (89%)
  local copies, waits for them, and re-layouts  8.36 us (9%)
  between operations  1.32 us (1%)
    pallas_call x1, Pallas kernels, on_device(): pl.pallas_call(functools.partial(kernel, ny, nz, nd), out_shape=(jax.Shap...  80.4 us
    unnamed x25, local copies, waits for them, and re-layouts  8.36 us

profile of v1, /device:TPU:1, one launch (start us, length us, event | category | flops | bytes accessed | tf_op | source)
XLA Modules:
  0.0 90.1 jit_solution(11459211655278138299)
XLA Ops:
  1.3 0.0 copy-start.8
  1.3 0.0 copy-start.9
  1.3 0.0 copy-start.10
  1.3 0.6 copy-done.8
  1.9 0.0 copy-done.9
  2.0 0.0 copy-done.10
  2.0 0.0 copy-start
  2.0 0.8 copy-done
  2.8 0.0 copy-start.1
  2.8 0.8 copy-done.1
  3.6 0.0 copy-start.2
  3.7 0.7 copy-done.2
  4.3 0.0 copy-start.3
  4.3 0.7 copy-done.3
  5.0 0.0 copy-start.4
  5.0 0.7 copy-done.4
  5.7 0.0 copy-start.5
  5.7 0.7 copy-done.5
  6.4 0.0 copy-start.6
  6.4 0.7 copy-done.6
  7.1 0.0 copy-start.7
  7.1 0.7 copy-done.7
  7.8 80.4 %mixer.1 = (bf16[128,256]{1,0:T(8,128)(2,1)S(1)}, f32[16,256]{1,0:T(8,128)S(1)}, f32[16,256]{1,0:T(8,128)S(1)}) custom-call(bf16[128,256]{1,0:T(8,128)(2,1)S(1)} %copy-done, bf16[128,256]{1,0:T(8,128)(2,1)S(1)} %copy-done.1, bf16[16,256]{1,0:T(8,128)(2,1)S(1)} %copy-done.2, bf16[16,256]{1,0:T(8,128)(2,1)S(1)} %copy-done.3, f32[1,32]{1,0:T(1,128)S(1)} %copy-done.8, ...), custom_call_target="tpu_custom_call" | custom-call | tf_op jit(solution)/shard_map/mixer/pallas_call | solution.py:446
  88.3 0.6 copy.19
  88.9 0.6 copy.20
  89.5 0.6 copy.21
Async XLA Ops:
  1.3 0.7 copy-start.8
  1.3 0.7 copy-start.9
  1.3 0.7 copy-start.10
  2.0 0.8 copy-start
  2.8 0.8 copy-start.1
  3.6 0.7 copy-start.2
  4.3 0.7 copy-start.3
  5.0 0.7 copy-start.4
  5.7 0.7 copy-start.5
  6.4 0.7 copy-start.6
  7.1 0.7 copy-start.7

commit v2 on v1

--- a/solution.py
+++ b/solution.py
@@ -41,6 +41,11 @@
     for _ in range(times):
         a = (a[0] * a[0] - a[1] * a[1], 2.0 * a[0] * a[1])
     return a
+
+
+def ring_order(n, far_first):
+    ks = sorted(range(1, n), key=lambda k: (min(k, n - k), k))
+    return ks[::-1] if far_first else ks
 
 
 def log2(n):
@@ -79,8 +84,9 @@
 
 def kernel(
     ny, nz, nd,
-    tok, cot, win, wout, rate, freq, slog, dr, di, rr, ri, skip,
+    slog, tok_h, cot_h, win_h, wout_h, rate_h, freq_h, dr_h, di_h, rr_h, ri_h, skip_h,
     o_tok, o_in, o_out,
+    tok, cot, win, wout, rate, freq, dr, di, rr, ri, skip,
     pk_own, aux_own, pk_z, aux_z, pk_y, aux_y,
     wa_in, wb_in, wa_out, wb_out,
     d_send, d_recv, b_send, b_recv,
@@ -89,7 +95,7 @@
     go_sa, go_sb, go_ra, go_rb, go_s2a, go_s2b, go_r2a, go_r2b,
     gi_sa, gi_sb, gi_ra, gi_rb, gi_s2a, gi_s2b, gi_r2a, gi_r2b,
     bre, bim, cre, cim, u_re, u_im, v_re, v_im,
-    ssem, rsem,
+    ssem, rsem, in1_sem, mix_sem, load_sem,
 ):
     sp, dp = lax.axis_index("sp"), lax.axis_index("dp")
     z, y = lax.div(sp, ny), lax.rem(sp, ny)
@@ -109,35 +115,45 @@
             return (j * ny + y, dp)
         return (sp, j)
 
-    def copy(phase, axis, k, src, dst):
-        j = lax.rem(here[axis] + k, size[axis])
+    def peer(axis, k):
+        return lax.rem(here[axis] + k, size[axis])
+
+    def copy(phase, axis, j, src, dst, recv_sem=None):
         return pltpu.make_async_remote_copy(
-            src_ref=src(j),
+            src_ref=src,
             dst_ref=dst,
-            send_sem=ssem.at[phase, k],
-            recv_sem=rsem.at[phase, k],
+            send_sem=ssem.at[phase],
+            recv_sem=rsem.at[phase] if recv_sem is None else recv_sem,
             device_id=device(axis, j),
             device_id_type=MESH,
         )
 
     sent = []
 
-    def send(phase, axis, src, dst):
-        for k in range(1, size[axis]):
-            copy(phase, axis, k, src, dst).start()
-        sent.append((phase, axis, src, dst))
-
-    def arrive(phase, axis, slot):
-        n = size[axis]
-        for k in range(1, n):
-            j = lax.rem(here[axis] + (n - k), n)
-            copy(phase, axis, k, lambda _: slot(j), slot(j)).wait_recv()
+    def send(phase, axis, src, dst, whole, sems=None):
+        for k in ring_order(size[axis], True):
+            j = peer(axis, k)
+            copy(phase, axis, j, src(j), dst, None if sems is None else sems(k)).start()
+        sent.append((phase, axis, whole))
+
+    def arrive(phase, axis, whole):
+        copy(phase, axis, peer(axis, 1), whole, whole).wait_recv()
 
     barrier = pltpu.get_barrier_semaphore()
     for axis in ("y", "z", "d"):
-        for k in range(1, size[axis]):
-            j = lax.rem(here[axis] + k, size[axis])
+        for k in ring_order(size[axis], True):
+            j = peer(axis, k)
             pl.semaphore_signal(barrier, inc=1, device_id=device(axis, j), device_id_type=MESH)
+
+    pairs = (
+        (rate_h, rate), (freq_h, freq), (dr_h, dr), (di_h, di), (rr_h, rr), (ri_h, ri),
+        (skip_h, skip), (win_h, win), (wout_h, wout), (tok_h, tok), (cot_h, cot),
+    )
+    loads = [pltpu.make_async_copy(a, b, load_sem.at[i]) for i, (a, b) in enumerate(pairs)]
+    for load in loads:
+        load.start()
+    for load in loads[:7]:
+        load.wait()
 
     tile_s = (iota((states, lanes), 0) == lax.rem(iota((states, lanes), 1), states)).astype(F32)
     wide = lambda ref: dot(jnp.broadcast_to(ref[...], (8, states)), tile_s, precision=HIGHEST)
@@ -174,53 +190,94 @@
 
     pl.semaphore_wait(barrier, (ny - 1) + (nz - 1) + (nd - 1))
 
-    send(IN_A1, "y", lambda j: win.at[:, 0:half], wa_in.at[z, y])
-    send(IN_B1, "z", lambda j: win.at[:, half:], wb_in.at[y, z])
-
     def param_copy(phase, k, src, dst):
-        j = lax.rem(z + k, nz)
-        return pltpu.make_async_remote_copy(
-            src_ref=src, dst_ref=dst, send_sem=ssem.at[phase, k], recv_sem=rsem.at[phase, 0],
-            device_id=(j * ny + y, dp), device_id_type=MESH,
-        )
+        return copy(phase, "z", peer("z", k), src, dst)
 
     @pl.when(z == dp)
     def _():
-        for k in range(1, nz):
+        for k in ring_order(nz, True):
             param_copy(PK_Z, k, pk_own, pk_z).start()
             param_copy(AUX_Z, k, aux_own, aux_z).start()
         pk_z[...] = pk_own[...]
         aux_z[...] = aux_own[...]
 
-    send(OUT_A1, "y", lambda j: wout.at[:, 0:half], wa_out.at[z, y])
-    send(OUT_B1, "z", lambda j: wout.at[:, half:], wb_out.at[y, z])
+    for load in loads[7:9]:
+        load.wait()
+    near, far = ring_order(ny, False), ring_order(nz, False)
+
+    def forward_a(j, src):
+        for k in ring_order(nz, True):
+            copy(IN_A2, "z", peer("z", k), src, wa_in.at[z, j]).start()
+
+    def forward_b(j, src):
+        for k in ring_order(ny, True):
+            copy(IN_B2, "y", peer("y", k), src, wb_in.at[y, j]).start()
+
+    left, right = win.at[:, 0:half], win.at[:, half:]
+    send(IN_A1, "y", lambda j: left, wa_in.at[z, y], wa_in.at[0, 0 : ny - 1], lambda k: in1_sem.at[0, k])
+    send(IN_B1, "z", lambda j: right, wb_in.at[y, z], wb_in.at[0, 0 : nz - 1], lambda k: in1_sem.at[1, k])
+    forward_a(y, left)
+    forward_b(z, right)
     wa_in[z, y] = win[:, 0:half]
     wb_in[y, z] = win[:, half:]
     wa_out[z, y] = wout[:, 0:half]
     wb_out[y, z] = wout[:, half:]
-
-    arrive(IN_A1, "y", lambda j: wa_in.at[z, j])
-    send(IN_A2, "z", lambda j: wa_in.at[z], wa_in.at[z])
-    arrive(IN_B1, "z", lambda j: wb_in.at[y, j])
-    send(IN_B2, "y", lambda j: wb_in.at[y], wb_in.at[y])
+    for i in range(max(ny, nz) - 1):
+        if i < ny - 1:
+            k = near[i]
+            j = peer("y", ny - k)
+            copy(IN_A1, "y", j, left, wa_in.at[z, j], in1_sem.at[0, k]).wait_recv()
+            forward_a(j, wa_in.at[z, j])
+        if i < nz - 1:
+            k = far[i]
+            j = peer("z", nz - k)
+            copy(IN_B1, "z", j, right, wb_in.at[y, j], in1_sem.at[1, k]).wait_recv()
+            forward_b(j, wb_in.at[y, j])
+        if i == 1 or max(ny, nz) == 2:
+            send(OUT_A1, "y", lambda j: wout.at[:, 0:half], wa_out.at[z, y], wa_out.at[0, 0 : ny - 1])
+            send(OUT_B1, "z", lambda j: wout.at[:, half:], wb_out.at[y, z], wb_out.at[0, 0 : nz - 1])
+    sent.append((IN_A2, "z", wa_in.at[0 : nz - 1]))
+    sent.append((IN_B2, "y", wb_in.at[0 : ny - 1]))
 
     @pl.when(z != dp)
     def _():
         param_copy(PK_Z, 1, pk_z, pk_z).wait_recv()
         param_copy(AUX_Z, 1, aux_z, aux_z).wait_recv()
 
-    send(PK_Y, "y", lambda j: pk_z, pk_y.at[y])
-    send(AUX_Y, "y", lambda j: aux_z, aux_y.at[y])
+    send(PK_Y, "y", lambda j: pk_z, pk_y.at[y], pk_y.at[0 : ny - 1])
+    send(AUX_Y, "y", lambda j: aux_z, aux_y.at[y], aux_y.at[0 : ny - 1])
     pk_y[y] = pk_z[...]
     aux_y[y] = aux_z[...]
 
-    arrive(OUT_A1, "y", lambda j: wa_out.at[z, j])
-    send(OUT_A2, "z", lambda j: wa_out.at[z], wa_out.at[z])
-    arrive(OUT_B1, "z", lambda j: wb_out.at[y, j])
-    send(OUT_B2, "y", lambda j: wb_out.at[y], wb_out.at[y])
-
-    arrive(PK_Y, "y", lambda j: pk_y.at[j])
-    arrive(AUX_Y, "y", lambda j: aux_y.at[j])
+    arrive(OUT_A1, "y", wa_out.at[0, 0 : ny - 1])
+    send(OUT_A2, "z", lambda j: wa_out.at[z], wa_out.at[z], wa_out.at[0 : nz - 1])
+    arrive(OUT_B1, "z", wb_out.at[0, 0 : nz - 1])
+    send(OUT_B2, "y", lambda j: wb_out.at[y], wb_out.at[y], wb_out.at[0 : ny - 1])
+
+    def weights_of(wa, wb, b):
+        left = wa[b].reshape(own_ch, half)
+        right = wb[:, b].reshape(own_ch, half)
+        return jnp.concatenate([left, right], axis=1)
+
+    def gathered(phase_a, phase_b, wa, wb):
+        arrive(phase_a, "z", wa.at[0 : nz - 1])
+        arrive(phase_b, "y", wb.at[0 : ny - 1])
+
+    def project(phase, act, wa, wb, out, recv):
+        for k in ring_order(nd, True):
+            j = peer("d", k)
+            out[j] = dot(act[...], weights_of(wa, wb, j), NT).astype(BF16)
+            copy(phase, "d", j, out.at[j], recv.at[dp]).start()
+        sent.append((phase, "d", recv.at[0 : nd - 1]))
+        recv[dp] = dot(act[...], weights_of(wa, wb, dp), NT).astype(BF16)
+
+    for load in loads[9:]:
+        load.wait()
+    gathered(IN_A2, IN_B2, wa_in, wb_in)
+    project(DRIVE, tok, wa_in, wb_in, d_send, d_recv)
+
+    arrive(PK_Y, "y", pk_y.at[0 : ny - 1])
+    arrive(AUX_Y, "y", aux_y.at[0 : ny - 1])
     packed = pk_y[...].reshape(own_ch, four)
     diag = lax.div(iota((own_ch, lanes), 0), per_group) == lax.div(iota((own_ch, lanes), 1), states)
     s_row, s_lane = iota((four, lanes), 0), lax.rem(iota((four, lanes), 1), states)
@@ -253,30 +310,13 @@
     dec_chunk = factor
     dec_row = square(dec_chunk, log2(ny))
 
-    def weights_of(wa, wb, b):
-        left = wa[b].reshape(own_ch, half)
-        right = wb[:, b].reshape(own_ch, half)
-        return jnp.concatenate([left, right], axis=1)
-
-    def gathered(phase_a, phase_b, wa, wb):
-        arrive(phase_a, "z", lambda j: wa.at[j])
-        arrive(phase_b, "y", lambda j: wb.at[j])
-
-    def project(act, wa, wb, out):
-        for b in range(nd):
-            out[b] = dot(act[...], weights_of(wa, wb, b), NT).astype(BF16)
-
     def total(recv):
         s = recv[0].astype(F32)
         for b in range(1, nd):
             s = s + recv[b].astype(F32)
         return s.astype(BF16)
 
-    gathered(IN_A2, IN_B2, wa_in, wb_in)
-    project(tok, wa_in, wb_in, d_send)
-    send(DRIVE, "d", lambda j: d_send.at[j], d_recv.at[dp])
-    d_recv[dp] = d_send[dp]
-    arrive(DRIVE, "d", lambda j: d_recv.at[j])
+    arrive(DRIVE, "d", d_recv.at[0 : nd - 1])
     x = total(d_recv)
 
     def carried(recv, n, me, decay, reverse):
@@ -312,21 +352,19 @@
     push = (dot(x, bre[...]), dot(x, bim[...]))
     final = summed(push, v_re, v_im, 1.0)
     put(f_own, final)
-    send(FWD_Y, "y", lambda j: f_own, f_recv.at[y])
+    send(FWD_Y, "y", lambda j: f_own, f_recv.at[y], f_recv.at[0 : ny - 1])
     put(f_recv.at[y], final)
     local = scan_rows(push, dec, False)
-    arrive(FWD_Y, "y", lambda j: f_recv.at[j])
+    arrive(FWD_Y, "y", f_recv.at[0 : ny - 1])
     enter_y, whole_y, power_y = carried(f_recv, ny, y, dec_chunk, False)
     put(t_own, whole_y)
-    send(FWD_Z, "z", lambda j: t_own, t_recv.at[z])
+    send(FWD_Z, "z", lambda j: t_own, t_recv.at[z], t_recv.at[0 : nz - 1])
     put(t_recv.at[z], whole_y)
 
     gathered(OUT_A2, OUT_B2, wa_out, wb_out)
-    project(cot, wa_out, wb_out, b_send)
-    send(BACK, "d", lambda j: b_send.at[j], b_recv.at[dp])
-    b_recv[dp] = b_send[dp]
-
-    arrive(FWD_Z, "z", lambda j: t_recv.at[j])
+    project(BACK, cot, wa_out, wb_out, b_send, b_recv)
+
+    arrive(FWD_Z, "z", t_recv.at[0 : nz - 1])
     enter_z, _, _ = carried(t_recv, nz, z, dec_row, False)
     far = cmul(power_y, enter_z)
     start = cmul(dec, (enter_y[0] + far[0], enter_y[1] + far[1]))
@@ -340,34 +378,46 @@
     gated = (mixed * half_up).astype(BF16)
     slope = half_up + 0.5 * mixed * (1.0 - th * th) * (c0 * (1.0 + 3.0 * 0.044715 * sq))
     gat_own[...] = gated
-    send(GATED, "d", lambda j: gat_own, gat_all.at[dp])
+    send(GATED, "d", lambda j: gat_own, gat_all.at[dp], gat_all.at[0 : nd - 1])
     gat_all[dp] = gated
 
-    arrive(BACK, "d", lambda j: b_recv.at[j])
+    arrive(BACK, "d", b_recv.at[0 : nd - 1])
     inner = slope * total(b_recv).astype(F32)
     inner_b = inner.astype(BF16)
     pulled = (dot(inner_b, cre[...]), -dot(inner_b, cim[...]))
     opening = summed(pulled, u_re, u_im, -1.0)
     put(a_own, opening)
-    send(BWD_Y, "y", lambda j: a_own, a_recv.at[y])
+    send(BWD_Y, "y", lambda j: a_own, a_recv.at[y], a_recv.at[0 : ny - 1])
     put(a_recv.at[y], opening)
     back_dec = conj(dec)
     local = scan_rows(pulled, back_dec, True)
-    arrive(BWD_Y, "y", lambda j: a_recv.at[j])
+    arrive(BWD_Y, "y", a_recv.at[0 : ny - 1])
     enter_y, whole_y, power_y = carried(a_recv, ny, y, conj(dec_chunk), True)
     put(q_own, whole_y)
-    send(BWD_Z, "z", lambda j: q_own, q_recv.at[z])
+    send(BWD_Z, "z", lambda j: q_own, q_recv.at[z], q_recv.at[0 : nz - 1])
     put(q_recv.at[z], whole_y)
 
-    def weight_grad(phase_a, phase_b, cols, act, sa, sb, ra, rb):
-        for b in range(nd):
-            part = dot(cols[b], act[...], TN).astype(BF16)
-            sa[b] = part[:, 0:half].reshape(ny, per_group, half)
-            sb[:, b] = part[:, half:].reshape(ny, per_group, half)
-        send(phase_a, "z", lambda j: sa.at[j], ra.at[z])
-        send(phase_b, "y", lambda j: sb.at[j], rb.at[y])
-        ra[z] = sa[z]
+    def weight_grad(phase_a, phase_b, b, cols, act, sa, sb, ra, rb):
+        part = dot(cols[b], act[...], TN).astype(BF16)
+        sa[b] = part[:, 0:half].reshape(ny, per_group, half)
+        sb[:, b] = part[:, half:].reshape(ny, per_group, half)
+
+        @pl.when(b != z)
+        def _():
+            copy(phase_a, "z", b, sa.at[b], ra.at[z]).start()
+
+        @pl.when(b == z)
+        def _():
+            ra[z] = sa[z]
+
+        for k in ring_order(ny, True):
+            j = peer("y", k)
+            copy(phase_b, "y", j, sb.at[j, b], rb.at[y, b]).start()
+
+    def all_blocks_sent(phase_a, phase_b, sb, ra, rb):
         rb[y] = sb[y]
+        sent.append((phase_a, "z", ra.at[0 : nz - 1]))
+        sent.append((phase_b, "y", rb.at[0 : ny - 1]))
 
     def reduced(recv, n):
         s = recv[0].astype(F32)
@@ -376,27 +426,29 @@
         return s
 
     def second_step(phase_a1, phase_b1, phase_a2, phase_b2, ra, rb, s2a, s2b, r2a, r2b):
-        arrive(phase_a1, "z", lambda j: ra.at[j])
+        arrive(phase_a1, "z", ra.at[0 : nz - 1])
         s2a[...] = reduced(ra, nz).astype(BF16)
-        send(phase_a2, "y", lambda j: s2a.at[j], r2a.at[y])
+        send(phase_a2, "y", lambda j: s2a.at[j], r2a.at[y], r2a.at[0 : ny - 1])
         r2a[y] = s2a[y]
-        arrive(phase_b1, "y", lambda j: rb.at[j])
+        arrive(phase_b1, "y", rb.at[0 : ny - 1])
         s2b[...] = reduced(rb, ny).astype(BF16)
-        send(phase_b2, "z", lambda j: s2b.at[j], r2b.at[z])
+        send(phase_b2, "z", lambda j: s2b.at[j], r2b.at[z], r2b.at[0 : nz - 1])
         r2b[z] = s2b[z]
 
     scale = (rows * ny * nz) ** -0.5
 
     def finish(phase_a2, phase_b2, r2a, r2b, out):
-        arrive(phase_a2, "y", lambda j: r2a.at[j])
-        arrive(phase_b2, "z", lambda j: r2b.at[j])
+        arrive(phase_a2, "y", r2a.at[0 : ny - 1])
+        arrive(phase_b2, "z", r2b.at[0 : nz - 1])
         out[:, 0:half] = reduced(r2a, ny) * scale
         out[:, half:] = reduced(r2b, nz) * scale
 
-    arrive(GATED, "d", lambda j: gat_all.at[j])
-    weight_grad(GO_A1, GO_B1, gat_all, cot, go_sa, go_sb, go_ra, go_rb)
-
-    arrive(BWD_Z, "z", lambda j: q_recv.at[j])
+    arrive(GATED, "d", gat_all.at[0 : nd - 1])
+    for b in range(nd):
+        weight_grad(GO_A1, GO_B1, b, gat_all, cot, go_sa, go_sb, go_ra, go_rb)
+    all_blocks_sent(GO_A1, GO_B1, go_sb, go_ra, go_rb)
+
+    arrive(BWD_Z, "z", q_recv.at[0 : nz - 1])
     enter_z, _, _ = carried(q_recv, nz, z, conj(dec_row), True)
     far = cmul(power_y, enter_z)
     start = cmul(back_dec, (enter_y[0] + far[0], enter_y[1] + far[1]))
@@ -404,29 +456,31 @@
     adj_re, adj_im = (local[0] + add[0]).astype(BF16), (local[1] + add[1]).astype(BF16)
     mix = (dot(adj_re, bre[...], NT) + dot(adj_im, bim[...], NT) + gain * inner).astype(BF16)
     mix_own[...] = mix
-    send(MIX, "d", lambda j: mix_own, mix_all.at[dp])
+    send(MIX, "d", lambda j: mix_own, mix_all.at[dp], mix_all.at[0 : nd - 1], lambda k: mix_sem.at[k])
     mix_all[dp] = mix
 
+    weight_grad(GI_A1, GI_B1, dp, mix_all, tok, gi_sa, gi_sb, gi_ra, gi_rb)
+    for k in ring_order(nd, False):
+        j = peer("d", nd - k)
+        copy(MIX, "d", j, mix_own, mix_all.at[j], mix_sem.at[k]).wait_recv()
+        weight_grad(GI_A1, GI_B1, j, mix_all, tok, gi_sa, gi_sb, gi_ra, gi_rb)
+    all_blocks_sent(GI_A1, GI_B1, gi_sb, gi_ra, gi_rb)
     second_step(GO_A1, GO_B1, GO_A2, GO_B2, go_ra, go_rb, go_s2a, go_s2b, go_r2a, go_r2b)
-    arrive(MIX, "d", lambda j: mix_all.at[j])
-    weight_grad(GI_A1, GI_B1, mix_all, tok, gi_sa, gi_sb, gi_ra, gi_rb)
     grad = dot(mix_all[0], weights_of(wa_in, wb_in, 0))
     for b in range(1, nd):
         grad = grad + dot(mix_all[b], weights_of(wa_in, wb_in, b))
     o_tok[...] = grad.astype(BF16)
+    second_step(GI_A1, GI_B1, GI_A2, GI_B2, gi_ra, gi_rb, gi_s2a, gi_s2b, gi_r2a, gi_r2b)
     finish(GO_A2, GO_B2, go_r2a, go_r2b, o_out)
-    second_step(GI_A1, GI_B1, GI_A2, GI_B2, gi_ra, gi_rb, gi_s2a, gi_s2b, gi_r2a, gi_r2b)
     finish(GI_A2, GI_B2, gi_r2a, gi_r2b, o_in)
 
     @pl.when(z == dp)
     def _():
-        for k in range(1, nz):
-            param_copy(PK_Z, k, pk_own, pk_z).wait_send()
-            param_copy(AUX_Z, k, aux_own, aux_z).wait_send()
-
-    for phase, axis, src, dst in sent:
-        for k in range(1, size[axis]):
-            copy(phase, axis, k, src, dst).wait_send()
+        param_copy(PK_Z, 1, pk_y.at[0 : nz - 1], pk_y.at[0 : nz - 1]).wait_send()
+        param_copy(AUX_Z, 1, aux_y.at[0 : nz - 1], aux_y.at[0 : nz - 1]).wait_send()
+
+    for phase, axis, whole in sent:
+        copy(phase, axis, peer(axis, 1), whole, whole).wait_send()
 
 
 def on_device(ny, nz, nd, tok, cot, win, wout, rate, freq, slog, dr, di, rr, ri, skip):
@@ -443,6 +497,8 @@
     ]
     most = max(ny, nz, nd)
     vm = pl.BlockSpec(memory_space=pltpu.VMEM)
+    drive = [jnp.swapaxes(a, 1, 2) for a in (dr, di)]
+    args = (tok, cot, win, wout, rate, freq, *drive, rr, ri, skip)
     return pl.pallas_call(
         functools.partial(kernel, ny, nz, nd),
         out_shape=(
@@ -450,9 +506,10 @@
             jax.ShapeDtypeStruct(win.shape, F32),
             jax.ShapeDtypeStruct(wout.shape, F32),
         ),
-        in_specs=[vm] * 6 + [pl.BlockSpec(memory_space=pltpu.SMEM)] + [vm] * 5,
+        in_specs=[pl.BlockSpec(memory_space=pltpu.SMEM)] + [pl.BlockSpec(memory_space=pltpu.HBM)] * len(args),
         out_specs=(vm, vm, vm),
         scratch_shapes=[
+            *[V(a.shape, a.dtype) for a in args],
             V((c, four), BF16), V((8, lanes), F32),
             V((c, four), BF16), V((8, lanes), F32),
             V((ny, c, four), BF16), V((ny, 8, lanes), F32),
@@ -469,14 +526,17 @@
             *grads, *grads,
             *[V((own_ch, lanes), BF16)] * 4,
             *[V((rows, lanes), F32)] * 4,
-            pltpu.SemaphoreType.DMA((PHASES, most)),
-            pltpu.SemaphoreType.DMA((PHASES, most)),
+            pltpu.SemaphoreType.DMA((PHASES,)),
+            pltpu.SemaphoreType.DMA((PHASES,)),
+            pltpu.SemaphoreType.DMA((2, most)),
+            pltpu.SemaphoreType.DMA((nd,)),
+            pltpu.SemaphoreType.DMA((len(args),)),
         ],
         compiler_params=pltpu.CompilerParams(
             collective_id=0, has_side_effects=True, vmem_limit_bytes=48 * 1024 * 1024
         ),
         name="mixer",
-    )(tok, cot, win, wout, rate, freq, slog, jnp.swapaxes(dr, 1, 2), jnp.swapaxes(di, 1, 2), rr, ri, skip)
+    )(slog, *[pltpu.with_memory_space_constraint(a, pltpu.HBM) for a in args])
 
 
 def solution(mesh):

time: 90.6 us -> 74.8 us (0.83)
  Pallas kernels: 80.4 us -> 71.5 us
  local copies, waits for them, and re-layouts: 8.36 us -> 1.84 us
    pallas_call x1, Pallas kernels: 80.4 us -> 71.5 us  [on_device(): pl.pallas_call(functools.partial(kernel, ny, nz, nd), out_shape=(jax.Shap...]
    unnamed x25 -> x3, local copies, waits for them, and re-layouts: 8.36 us -> 1.84 us
where the time goes in v2:
time: 74.8 us; the launch traced here: 74.6 us
  Pallas kernels  71.5 us (96%)
  local copies, waits for them, and re-layouts  1.84 us (2%)
  between operations  1.29 us (2%)
    pallas_call x1, Pallas kernels, on_device(): pl.pallas_call(functools.partial(kernel, ny, nz, nd), out_shape=(jax.Shap...  71.5 us
    unnamed x3, local copies, waits for them, and re-layouts  1.84 us

profile of v2, /device:TPU:1, one launch (start us, length us, event | category | flops | bytes accessed | tf_op | source)
XLA Modules:
  0.0 74.6 jit_solution(5775248938994028217)
XLA Ops:
  1.3 71.5 %mixer.1 = (bf16[128,256]{1,0:T(8,128)(2,1)S(1)}, f32[16,256]{1,0:T(8,128)S(1)}, f32[16,256]{1,0:T(8,128)S(1)}) custom-call(f32[1]{0:T(128)S(6)} %copy.18.slog, bf16[128,256]{1,0:T(8,128)(2,1)} %tok_h.1, bf16[128,256]{1,0:T(8,128)(2,1)} %cot_h.1, bf16[16,256]{1,0:T(8,128)(2,1)} %win_h.1, bf16[16,256]{1,0:T(8,128)(2,1)} %wout_h.1, f32[1,32]{1,0:T(1,128)} %rate_h.1, ...), custom_call_target="tpu_custom_call" | custom-call | tf_op jit(solution)/shard_map/mixer/pallas_call | solution.py:502
  72.8 0.6 copy.19
  73.4 0.6 copy.20
  74.0 0.6 copy.21

commit v3 on v2

--- a/solution.py
+++ b/solution.py
@@ -16,9 +16,9 @@
 (
     IN_A1, IN_B1, IN_A2, IN_B2, OUT_A1, OUT_B1, OUT_A2, OUT_B2,
     PK_Z, AUX_Z, PK_Y, AUX_Y, DRIVE, BACK, FWD_Y, FWD_Z, BWD_Y, BWD_Z,
-    GATED, MIX, GO_A1, GO_B1, GO_A2, GO_B2, GI_A1, GI_B1, GI_A2, GI_B2,
-) = range(28)
-PHASES = 28
+    GATED, MIX, GO_A1, GO_B1, GO_A2, GO_B2, GI_A1, GI_B1, GI_A2, GI_B2, GO_HA, GO_HB, GI_HA, GI_HB,
+) = range(32)
+PHASES = 32
 
 NN = (((1,), (0,)), ((), ()))
 NT = (((1,), (1,)), ((), ()))
@@ -46,6 +46,18 @@
 def ring_order(n, far_first):
     ks = sorted(range(1, n), key=lambda k: (min(k, n - k), k))
     return ks[::-1] if far_first else ks
+
+
+def slots(n):
+    held = [0] + ring_order(n, False)
+    return held, {k: i for i, k in enumerate(held)}
+
+
+def slot_of(n, k):
+    if n != 8:
+        return k
+    late = lax.div(k, 5)
+    return (2 * k - 1) * (1 - late) + (16 - 2 * k) * late + 1 - lax.div(k + 7, 8)
 
 
 def log2(n):
@@ -92,10 +104,10 @@
     d_send, d_recv, b_send, b_recv,
     f_own, f_recv, t_own, t_recv, a_own, a_recv, q_own, q_recv,
     gat_own, gat_all, mix_own, mix_all,
-    go_sa, go_sb, go_ra, go_rb, go_s2a, go_s2b, go_r2a, go_r2b,
-    gi_sa, gi_sb, gi_ra, gi_rb, gi_s2a, gi_s2b, gi_r2a, gi_r2b,
+    go_sa, go_sb, go_ha, go_hb, go_ra, go_rb, go_s2a, go_s2b, go_r2a, go_r2b,
+    gi_sa, gi_sb, gi_ha, gi_hb, gi_ra, gi_rb, gi_s2a, gi_s2b, gi_r2a, gi_r2b,
     bre, bim, cre, cim, u_re, u_im, v_re, v_im,
-    ssem, rsem, in1_sem, mix_sem, load_sem,
+    ssem, rsem, in1_sem, in2_sem, mix_sem, load_sem,
 ):
     sp, dp = lax.axis_index("sp"), lax.axis_index("dp")
     z, y = lax.div(sp, ny), lax.rem(sp, ny)
@@ -107,6 +119,10 @@
     own_ch = ny * per_group
     lanes = ny * states
     half = win.shape[1] // 2
+    core = lax.rem(dp, 2)
+    _, at_y = slots(ny)
+    _, at_z = slots(nz)
+    slot = {"y": lambda k: at_y[k % ny], "z": lambda k: at_z[k % nz]}
 
     def device(axis, j):
         if axis == "y":
@@ -132,12 +148,19 @@
 
     def send(phase, axis, src, dst, whole, sems=None):
         for k in ring_order(size[axis], True):
-            j = peer(axis, k)
-            copy(phase, axis, j, src(j), dst, None if sems is None else sems(k)).start()
+            copy(phase, axis, peer(axis, k), src(k), dst(k), None if sems is None else sems(k)).start()
         sent.append((phase, axis, whole))
 
     def arrive(phase, axis, whole):
         copy(phase, axis, peer(axis, 1), whole, whole).wait_recv()
+
+    pairs = (
+        (win_h, win), (wout_h, wout), (rate_h, rate), (freq_h, freq), (dr_h, dr), (di_h, di), (rr_h, rr),
+        (ri_h, ri), (skip_h, skip), (tok_h, tok), (cot_h, cot),
+    )
+    loads = [pltpu.make_async_copy(a, b, load_sem.at[i]) for i, (a, b) in enumerate(pairs)]
+    for load in loads:
+        load.start()
 
     barrier = pltpu.get_barrier_semaphore()
     for axis in ("y", "z", "d"):
@@ -145,14 +168,43 @@
             j = peer(axis, k)
             pl.semaphore_signal(barrier, inc=1, device_id=device(axis, j), device_id_type=MESH)
 
-    pairs = (
-        (rate_h, rate), (freq_h, freq), (dr_h, dr), (di_h, di), (rr_h, rr), (ri_h, ri),
-        (skip_h, skip), (win_h, win), (wout_h, wout), (tok_h, tok), (cot_h, cot),
+    pl.semaphore_wait(barrier, (ny - 1) + (nz - 1) + (nd - 1))
+
+    for load in loads[:2]:
+        load.wait()
+
+    def parts(n):
+        return ((0, 1), (1, 5), (5, 8)) if n == 8 else ((0, 1), (1, n))
+
+    def part_of(n, at):
+        return [a <= at < b for a, b in parts(n)].index(True)
+
+    def spread(phase, axis, w, src, a, b, sems=None):
+        for k in ring_order(size[axis], True):
+            at = slot[axis](-k)
+            dst = w.at[at, a] if b is None else w.at[at, a:b]
+            copy(phase, axis, peer(axis, k), src, dst, None if sems is None else sems(at)).start()
+
+    def gathered(phase, axis, w):
+        arrive(phase, axis, w.at[1:])
+        sent.append((phase, axis, w.at[1:]))
+
+    left, right = win.at[:, 0:half], win.at[:, half:]
+    send(
+        IN_A1, "y", lambda k: left, lambda k: wa_in.at[0, at_y[-k % ny]], wa_in.at[0, 1:],
+        lambda k: in1_sem.at[0, part_of(ny, at_y[-k % ny])],
     )
-    loads = [pltpu.make_async_copy(a, b, load_sem.at[i]) for i, (a, b) in enumerate(pairs)]
-    for load in loads:
-        load.start()
-    for load in loads[:7]:
+    send(
+        IN_B1, "z", lambda k: right, lambda k: wb_in.at[0, at_z[-k % nz]], wb_in.at[0, 1:],
+        lambda k: in1_sem.at[1, part_of(nz, at_z[-k % nz])],
+    )
+    spread(IN_A2, "z", wa_in, left, 0, None, lambda at: in2_sem.at[0, at])
+    spread(IN_B2, "y", wb_in, right, 0, None, lambda at: in2_sem.at[1, 0])
+    wa_in[0, 0] = win[:, 0:half]
+    wb_in[0, 0] = win[:, half:]
+    wa_out[0, 0] = wout[:, 0:half]
+    wb_out[0, 0] = wout[:, half:]
+    for load in loads[2:9]:
         load.wait()
 
     tile_s = (iota((states, lanes), 0) == lax.rem(iota((states, lanes), 1), states)).astype(F32)
@@ -188,8 +240,6 @@
         + dot(ri[0], sel_d, NN, HIGHEST)
     ).astype(BF16)
 
-    pl.semaphore_wait(barrier, (ny - 1) + (nz - 1) + (nd - 1))
-
     def param_copy(phase, k, src, dst):
         return copy(phase, "z", peer("z", k), src, dst)
 
@@ -201,67 +251,43 @@
         pk_z[...] = pk_own[...]
         aux_z[...] = aux_own[...]
 
-    for load in loads[7:9]:
-        load.wait()
-    near, far = ring_order(ny, False), ring_order(nz, False)
-
-    def forward_a(j, src):
-        for k in ring_order(nz, True):
-            copy(IN_A2, "z", peer("z", k), src, wa_in.at[z, j]).start()
-
-    def forward_b(j, src):
-        for k in ring_order(ny, True):
-            copy(IN_B2, "y", peer("y", k), src, wb_in.at[y, j]).start()
-
-    left, right = win.at[:, 0:half], win.at[:, half:]
-    send(IN_A1, "y", lambda j: left, wa_in.at[z, y], wa_in.at[0, 0 : ny - 1], lambda k: in1_sem.at[0, k])
-    send(IN_B1, "z", lambda j: right, wb_in.at[y, z], wb_in.at[0, 0 : nz - 1], lambda k: in1_sem.at[1, k])
-    forward_a(y, left)
-    forward_b(z, right)
-    wa_in[z, y] = win[:, 0:half]
-    wb_in[y, z] = win[:, half:]
-    wa_out[z, y] = wout[:, 0:half]
-    wb_out[y, z] = wout[:, half:]
-    for i in range(max(ny, nz) - 1):
-        if i < ny - 1:
-            k = near[i]
-            j = peer("y", ny - k)
-            copy(IN_A1, "y", j, left, wa_in.at[z, j], in1_sem.at[0, k]).wait_recv()
-            forward_a(j, wa_in.at[z, j])
-        if i < nz - 1:
-            k = far[i]
-            j = peer("z", nz - k)
-            copy(IN_B1, "z", j, right, wb_in.at[y, j], in1_sem.at[1, k]).wait_recv()
-            forward_b(j, wb_in.at[y, j])
-        if i == 1 or max(ny, nz) == 2:
-            send(OUT_A1, "y", lambda j: wout.at[:, 0:half], wa_out.at[z, y], wa_out.at[0, 0 : ny - 1])
-            send(OUT_B1, "z", lambda j: wout.at[:, half:], wb_out.at[y, z], wb_out.at[0, 0 : nz - 1])
-    sent.append((IN_A2, "z", wa_in.at[0 : nz - 1]))
-    sent.append((IN_B2, "y", wb_in.at[0 : ny - 1]))
+    def forward(part):
+        if part < len(parts(ny)):
+            a, b = parts(ny)[part]
+            own = wa_in.at[0, a:b]
+            copy(IN_A1, "y", peer("y", 1), own, own, in1_sem.at[0, part]).wait_recv()
+            spread(IN_A2, "z", wa_in, own, a, b, lambda at: in2_sem.at[0, at])
+        if part < len(parts(nz)):
+            a, b = parts(nz)[part]
+            own = wb_in.at[0, a:b]
+            copy(IN_B1, "z", peer("z", 1), own, own, in1_sem.at[1, part]).wait_recv()
+            spread(IN_B2, "y", wb_in, own, a, b, lambda at: in2_sem.at[1, part])
+
+    forward(1)
+    send(OUT_A1, "y", lambda k: wout.at[:, 0:half], lambda k: wa_out.at[0, at_y[-k % ny]], wa_out.at[0, 1:])
+    send(OUT_B1, "z", lambda k: wout.at[:, half:], lambda k: wb_out.at[0, at_z[-k % nz]], wb_out.at[0, 1:])
+    if max(ny, nz) > 2:
+        forward(2)
 
     @pl.when(z != dp)
     def _():
         param_copy(PK_Z, 1, pk_z, pk_z).wait_recv()
         param_copy(AUX_Z, 1, aux_z, aux_z).wait_recv()
 
-    send(PK_Y, "y", lambda j: pk_z, pk_y.at[y], pk_y.at[0 : ny - 1])
-    send(AUX_Y, "y", lambda j: aux_z, aux_y.at[y], aux_y.at[0 : ny - 1])
+    send(PK_Y, "y", lambda k: pk_z, lambda k: pk_y.at[y], pk_y.at[1:])
+    send(AUX_Y, "y", lambda k: aux_z, lambda k: aux_y.at[y], aux_y.at[1:])
     pk_y[y] = pk_z[...]
     aux_y[y] = aux_z[...]
 
-    arrive(OUT_A1, "y", wa_out.at[0, 0 : ny - 1])
-    send(OUT_A2, "z", lambda j: wa_out.at[z], wa_out.at[z], wa_out.at[0 : nz - 1])
-    arrive(OUT_B1, "z", wb_out.at[0, 0 : nz - 1])
-    send(OUT_B2, "y", lambda j: wb_out.at[y], wb_out.at[y], wb_out.at[0 : ny - 1])
 
     def weights_of(wa, wb, b):
-        left = wa[b].reshape(own_ch, half)
-        right = wb[:, b].reshape(own_ch, half)
+        return weights_at(wa, wb, slot_of(nz, lax.rem(b - z + nz, nz)))
+
+    def weights_at(wa, wb, at):
+        place = [slot_of(ny, lax.rem(g - y + ny, ny)) for g in range(ny)]
+        left = jnp.concatenate([wa[at, i] for i in place], axis=0)
+        right = jnp.concatenate([wb[i, at] for i in place], axis=0)
         return jnp.concatenate([left, right], axis=1)
-
-    def gathered(phase_a, phase_b, wa, wb):
-        arrive(phase_a, "z", wa.at[0 : nz - 1])
-        arrive(phase_b, "y", wb.at[0 : ny - 1])
 
     def project(phase, act, wa, wb, out, recv):
         for k in ring_order(nd, True):
@@ -273,8 +299,33 @@
 
     for load in loads[9:]:
         load.wait()
-    gathered(IN_A2, IN_B2, wa_in, wb_in)
-    project(DRIVE, tok, wa_in, wb_in, d_send, d_recv)
+    for at in range(nz):
+        for part, (a, e) in enumerate(parts(nz)):
+            if at == a:
+                got = wb_in.at[1:, a:e]
+                with jax.named_scope("IN_B%d" % at):
+                    copy(IN_B2, "y", peer("y", 1), got, got, in2_sem.at[1, part]).wait_recv()
+        if at:
+            with jax.named_scope("IN_A%d" % at):
+                copy(IN_A2, "z", peer("z", 1), wa_in.at[at], wa_in.at[at], in2_sem.at[0, at]).wait_recv()
+        b = peer("z", slots(nz)[0][at])
+        d_send[b] = dot(tok[...], weights_at(wa_in, wb_in, at), NT).astype(BF16)
+
+        @pl.when(b != dp)
+        def _():
+            copy(DRIVE, "d", b, d_send.at[b], d_recv.at[dp]).start()
+
+        @pl.when(b == dp)
+        def _():
+            d_recv[dp] = d_send[dp]
+
+    sent.append((IN_A2, "z", wa_in.at[1:]))
+    sent.append((IN_B2, "y", wb_in.at[1:]))
+    sent.append((DRIVE, "d", d_recv.at[0 : nd - 1]))
+    arrive(OUT_A1, "y", wa_out.at[0, 1:])
+    spread(OUT_A2, "z", wa_out, wa_out.at[0, 0:ny], 0, ny)
+    arrive(OUT_B1, "z", wb_out.at[0, 1:])
+    spread(OUT_B2, "y", wb_out, wb_out.at[0, 0:nz], 0, nz)
 
     arrive(PK_Y, "y", pk_y.at[0 : ny - 1])
     arrive(AUX_Y, "y", aux_y.at[0 : ny - 1])
@@ -352,17 +403,18 @@
     push = (dot(x, bre[...]), dot(x, bim[...]))
     final = summed(push, v_re, v_im, 1.0)
     put(f_own, final)
-    send(FWD_Y, "y", lambda j: f_own, f_recv.at[y], f_recv.at[0 : ny - 1])
+    send(FWD_Y, "y", lambda k: f_own, lambda k: f_recv.at[y], f_recv.at[0 : ny - 1])
     put(f_recv.at[y], final)
     local = scan_rows(push, dec, False)
+    gathered(OUT_A2, "z", wa_out)
+    gathered(OUT_B2, "y", wb_out)
+    project(BACK, cot, wa_out, wb_out, b_send, b_recv)
+
     arrive(FWD_Y, "y", f_recv.at[0 : ny - 1])
     enter_y, whole_y, power_y = carried(f_recv, ny, y, dec_chunk, False)
     put(t_own, whole_y)
-    send(FWD_Z, "z", lambda j: t_own, t_recv.at[z], t_recv.at[0 : nz - 1])
+    send(FWD_Z, "z", lambda k: t_own, lambda k: t_recv.at[z], t_recv.at[0 : nz - 1])
     put(t_recv.at[z], whole_y)
-
-    gathered(OUT_A2, OUT_B2, wa_out, wb_out)
-    project(BACK, cot, wa_out, wb_out, b_send, b_recv)
 
     arrive(FWD_Z, "z", t_recv.at[0 : nz - 1])
     enter_z, _, _ = carried(t_recv, nz, z, dec_row, False)
@@ -377,47 +429,56 @@
     half_up = 0.5 * (1.0 + th)
     gated = (mixed * half_up).astype(BF16)
     slope = half_up + 0.5 * mixed * (1.0 - th * th) * (c0 * (1.0 + 3.0 * 0.044715 * sq))
-    gat_own[...] = gated
-    send(GATED, "d", lambda j: gat_own, gat_all.at[dp], gat_all.at[0 : nd - 1])
-    gat_all[dp] = gated
-
     arrive(BACK, "d", b_recv.at[0 : nd - 1])
     inner = slope * total(b_recv).astype(F32)
     inner_b = inner.astype(BF16)
     pulled = (dot(inner_b, cre[...]), -dot(inner_b, cim[...]))
     opening = summed(pulled, u_re, u_im, -1.0)
     put(a_own, opening)
-    send(BWD_Y, "y", lambda j: a_own, a_recv.at[y], a_recv.at[0 : ny - 1])
+    send(BWD_Y, "y", lambda k: a_own, lambda k: a_recv.at[y], a_recv.at[0 : ny - 1])
     put(a_recv.at[y], opening)
+    gat_own[...] = gated
+    send(GATED, "d", lambda k: gat_own, lambda k: gat_all.at[dp], gat_all.at[0 : nd - 1])
+    gat_all[dp] = gated
     back_dec = conj(dec)
     local = scan_rows(pulled, back_dec, True)
     arrive(BWD_Y, "y", a_recv.at[0 : ny - 1])
     enter_y, whole_y, power_y = carried(a_recv, ny, y, conj(dec_chunk), True)
     put(q_own, whole_y)
-    send(BWD_Z, "z", lambda j: q_own, q_recv.at[z], q_recv.at[0 : nz - 1])
+    send(BWD_Z, "z", lambda k: q_own, lambda k: q_recv.at[z], q_recv.at[0 : nz - 1])
     put(q_recv.at[z], whole_y)
 
-    def weight_grad(phase_a, phase_b, b, cols, act, sa, sb, ra, rb):
+    def block_of_grad(b, cols, act, sa, sb):
         part = dot(cols[b], act[...], TN).astype(BF16)
         sa[b] = part[:, 0:half].reshape(ny, per_group, half)
         sb[:, b] = part[:, half:].reshape(ny, per_group, half)
 
-        @pl.when(b != z)
-        def _():
-            copy(phase_a, "z", b, sa.at[b], ra.at[z]).start()
-
-        @pl.when(b == z)
-        def _():
-            ra[z] = sa[z]
-
-        for k in ring_order(ny, True):
-            j = peer("y", k)
-            copy(phase_b, "y", j, sb.at[j, b], rb.at[y, b]).start()
-
-    def all_blocks_sent(phase_a, phase_b, sb, ra, rb):
-        rb[y] = sb[y]
-        sent.append((phase_a, "z", ra.at[0 : nz - 1]))
-        sent.append((phase_b, "y", rb.at[0 : ny - 1]))
+    def hand_on(phase, phase_h, axis, s, h, r):
+        if size[axis] != 8:
+            for k in ring_order(size[axis], True):
+                copy(phase, axis, peer(axis, k), s.at[peer(axis, k)], r.at[slot[axis](-k)]).start()
+            sent.append((phase, axis, r.at[1:]))
+        else:
+            copy(phase_h, axis, peer(axis, 2 + 4 * core), s.at[peer(axis, 4)], h.at[2]).start()
+            copy(phase_h, axis, peer(axis, 1), s.at[peer(axis, 3)], h.at[0]).start()
+            copy(phase_h, axis, peer(axis, 7), s.at[peer(axis, 5)], h.at[1]).start()
+            copy(phase, axis, peer(axis, 1), s.at[peer(axis, 1)], r.at[1]).start()
+            copy(phase, axis, peer(axis, 7), s.at[peer(axis, 7)], r.at[2]).start()
+        r[0] = s[here[axis]]
+
+    def add_to(s, j, part):
+        s[j] = (s[j].astype(F32) + part.astype(F32)).astype(BF16)
+
+    def pass_on(phase, phase_h, axis, s, h, r):
+        if size[axis] == 8:
+            arrive(phase_h, axis, h)
+            add_to(s, peer(axis, 2), h[0])
+            add_to(s, peer(axis, 6), h[1])
+            add_to(s, peer(axis, 2 + 4 * core), h[2])
+            copy(phase, axis, peer(axis, 2), s.at[peer(axis, 2)], r.at[3]).start()
+            copy(phase, axis, peer(axis, 6), s.at[peer(axis, 6)], r.at[4]).start()
+            sent.append((phase_h, axis, h))
+            sent.append((phase, axis, r.at[1:]))
 
     def reduced(recv, n):
         s = recv[0].astype(F32)
@@ -426,14 +487,14 @@
         return s
 
     def second_step(phase_a1, phase_b1, phase_a2, phase_b2, ra, rb, s2a, s2b, r2a, r2b):
-        arrive(phase_a1, "z", ra.at[0 : nz - 1])
-        s2a[...] = reduced(ra, nz).astype(BF16)
-        send(phase_a2, "y", lambda j: s2a.at[j], r2a.at[y], r2a.at[0 : ny - 1])
-        r2a[y] = s2a[y]
-        arrive(phase_b1, "y", rb.at[0 : ny - 1])
-        s2b[...] = reduced(rb, ny).astype(BF16)
-        send(phase_b2, "z", lambda j: s2b.at[j], r2b.at[z], r2b.at[0 : nz - 1])
-        r2b[z] = s2b[z]
+        arrive(phase_a1, "z", ra.at[1:])
+        s2a[...] = reduced(ra, ra.shape[0]).astype(BF16)
+        send(phase_a2, "y", lambda k: s2a.at[peer("y", k)], lambda k: r2a.at[at_y[-k % ny]], r2a.at[1:])
+        r2a[0] = s2a[y]
+        arrive(phase_b1, "y", rb.at[1:])
+        s2b[...] = reduced(rb, rb.shape[0]).astype(BF16)
+        send(phase_b2, "z", lambda k: s2b.at[peer("z", k)], lambda k: r2b.at[at_z[-k % nz]], r2b.at[1:])
+        r2b[0] = s2b[z]
 
     scale = (rows * ny * nz) ** -0.5
 
@@ -445,8 +506,9 @@
 
     arrive(GATED, "d", gat_all.at[0 : nd - 1])
     for b in range(nd):
-        weight_grad(GO_A1, GO_B1, b, gat_all, cot, go_sa, go_sb, go_ra, go_rb)
-    all_blocks_sent(GO_A1, GO_B1, go_sb, go_ra, go_rb)
+        block_of_grad(b, gat_all, cot, go_sa, go_sb)
+    hand_on(GO_A1, GO_HA, "z", go_sa, go_ha, go_ra)
+    hand_on(GO_B1, GO_HB, "y", go_sb, go_hb, go_rb)
 
     arrive(BWD_Z, "z", q_recv.at[0 : nz - 1])
     enter_z, _, _ = carried(q_recv, nz, z, conj(dec_row), True)
@@ -456,20 +518,25 @@
     adj_re, adj_im = (local[0] + add[0]).astype(BF16), (local[1] + add[1]).astype(BF16)
     mix = (dot(adj_re, bre[...], NT) + dot(adj_im, bim[...], NT) + gain * inner).astype(BF16)
     mix_own[...] = mix
-    send(MIX, "d", lambda j: mix_own, mix_all.at[dp], mix_all.at[0 : nd - 1], lambda k: mix_sem.at[k])
+    send(MIX, "d", lambda k: mix_own, lambda k: mix_all.at[dp], mix_all.at[0 : nd - 1], lambda k: mix_sem.at[k])
     mix_all[dp] = mix
 
-    weight_grad(GI_A1, GI_B1, dp, mix_all, tok, gi_sa, gi_sb, gi_ra, gi_rb)
+    pass_on(GO_A1, GO_HA, "z", go_sa, go_ha, go_ra)
+    pass_on(GO_B1, GO_HB, "y", go_sb, go_hb, go_rb)
+    block_of_grad(dp, mix_all, tok, gi_sa, gi_sb)
     for k in ring_order(nd, False):
         j = peer("d", nd - k)
         copy(MIX, "d", j, mix_own, mix_all.at[j], mix_sem.at[k]).wait_recv()
-        weight_grad(GI_A1, GI_B1, j, mix_all, tok, gi_sa, gi_sb, gi_ra, gi_rb)
-    all_blocks_sent(GI_A1, GI_B1, gi_sb, gi_ra, gi_rb)
+        block_of_grad(j, mix_all, tok, gi_sa, gi_sb)
+    hand_on(GI_A1, GI_HA, "z", gi_sa, gi_ha, gi_ra)
+    hand_on(GI_B1, GI_HB, "y", gi_sb, gi_hb, gi_rb)
     second_step(GO_A1, GO_B1, GO_A2, GO_B2, go_ra, go_rb, go_s2a, go_s2b, go_r2a, go_r2b)
     grad = dot(mix_all[0], weights_of(wa_in, wb_in, 0))
     for b in range(1, nd):
         grad = grad + dot(mix_all[b], weights_of(wa_in, wb_in, b))
     o_tok[...] = grad.astype(BF16)
+    pass_on(GI_A1, GI_HA, "z", gi_sa, gi_ha, gi_ra)
+    pass_on(GI_B1, GI_HB, "y", gi_sb, gi_hb, gi_rb)
     second_step(GI_A1, GI_B1, GI_A2, GI_B2, gi_ra, gi_rb, gi_s2a, gi_s2b, gi_r2a, gi_r2b)
     finish(GO_A2, GO_B2, go_r2a, go_r2b, o_out)
     finish(GI_A2, GI_B2, gi_r2a, gi_r2b, o_in)
@@ -481,6 +548,14 @@
 
     for phase, axis, whole in sent:
         copy(phase, axis, peer(axis, 1), whole, whole).wait_send()
+
+
+def store(a, b, c, out_a, out_b, out_c, sem):
+    copies = [pltpu.make_async_copy(s, d, sem.at[i]) for i, (s, d) in enumerate(((a, out_a), (b, out_b), (c, out_c)))]
+    for copy in copies:
+        copy.start()
+    for copy in copies:
+        copy.wait()
 
 
 def on_device(ny, nz, nd, tok, cot, win, wout, rate, freq, slog, dr, di, rr, ri, skip):
@@ -489,17 +564,18 @@
     states, c = rate.shape[1], skip.shape[1]
     own_ch, lanes, four = ny * c, ny * states, 4 * states
     V = pltpu.VMEM
-    grads = [
+    come = lambda n: 5 if n == 8 else n
+    relayed = [
         V((nz, ny, c, half), BF16), V((ny, nz, c, half), BF16),
-        V((nz, ny, c, half), BF16), V((ny, nz, c, half), BF16),
+        V((3, ny, c, half), BF16), V((3, nz, c, half), BF16),
+        V((come(nz), ny, c, half), BF16), V((come(ny), nz, c, half), BF16),
         V((ny, c, half), BF16), V((nz, c, half), BF16),
         V((ny, c, half), BF16), V((nz, c, half), BF16),
     ]
-    most = max(ny, nz, nd)
     vm = pl.BlockSpec(memory_space=pltpu.VMEM)
     drive = [jnp.swapaxes(a, 1, 2) for a in (dr, di)]
     args = (tok, cot, win, wout, rate, freq, *drive, rr, ri, skip)
-    return pl.pallas_call(
+    outs = pl.pallas_call(
         functools.partial(kernel, ny, nz, nd),
         out_shape=(
             jax.ShapeDtypeStruct((rows, cols), BF16),
@@ -523,12 +599,13 @@
             V((2, lanes), F32), V((nz, 2, lanes), F32),
             V((rows, own_ch), BF16), V((nd, rows, own_ch), BF16),
             V((rows, own_ch), BF16), V((nd, rows, own_ch), BF16),
-            *grads, *grads,
+            *relayed, *relayed,
             *[V((own_ch, lanes), BF16)] * 4,
             *[V((rows, lanes), F32)] * 4,
             pltpu.SemaphoreType.DMA((PHASES,)),
             pltpu.SemaphoreType.DMA((PHASES,)),
-            pltpu.SemaphoreType.DMA((2, most)),
+            pltpu.SemaphoreType.DMA((2, 3)),
+            pltpu.SemaphoreType.DMA((2, 8)),
             pltpu.SemaphoreType.DMA((nd,)),
             pltpu.SemaphoreType.DMA((len(args),)),
         ],
@@ -537,6 +614,15 @@
         ),
         name="mixer",
     )(slog, *[pltpu.with_memory_space_constraint(a, pltpu.HBM) for a in args])
+    return pl.pallas_call(
+        store,
+        out_shape=tuple(jax.ShapeDtypeStruct(o.shape, o.dtype) for o in outs),
+        in_specs=[vm] * 3,
+        out_specs=(pl.BlockSpec(memory_space=pltpu.HBM),) * 3,
+        scratch_shapes=[pltpu.SemaphoreType.DMA((3,))],
+        compiler_params=pltpu.CompilerParams(vmem_limit_bytes=8 * 1024 * 1024),
+        name="store",
+    )(*outs)
 
 
 def solution(mesh):

time: 74.8 us -> 71.5 us (0.956); the launches traced: 74.6 us -> 70.6 us
  Pallas kernels: 71.5 us -> 69.3 us
  local copies, waits for them, and re-layouts: 1.84 us -> 0 us
    pallas_call x1, Pallas kernels: 71.5 us -> 68.6 us  [on_device(): pl.pallas_call(functools.partial(kernel, ny, nz, nd), out_shape=(jax.Shap...]
    unnamed x3 -> x0, local copies, waits for them, and re-layouts: 1.84 us -> none
where the time goes in v3:
time: 71.5 us; the launch traced here: 70.6 us
  Pallas kernels  69.3 us (97%)
  between operations  1.29 us (2%)
    pallas_call x1, Pallas kernels, on_device(): pl.pallas_call(functools.partial(kernel, ny, nz, nd), out_shape=(jax.Shap...  68.6 us

profile of v3, /device:TPU:1, one launch (start us, length us, event | category | flops | bytes accessed | tf_op | source)
XLA Modules:
  0.0 70.6 jit_solution(14959431128148453606)
XLA Ops:
  1.3 68.6 %mixer.1 = (bf16[128,256]{1,0:T(8,128)(2,1)S(1)}, f32[16,256]{1,0:T(8,128)S(1)}, f32[16,256]{1,0:T(8,128)S(1)}) custom-call(f32[1]{0:T(128)S(6)} %copy.15.slog, bf16[128,256]{1,0:T(8,128)(2,1)} %tok_h.1, bf16[128,256]{1,0:T(8,128)(2,1)} %cot_h.1, bf16[16,256]{1,0:T(8,128)(2,1)} %win_h.1, bf16[16,256]{1,0:T(8,128)(2,1)} %wout_h.1, f32[1,32]{1,0:T(1,128)} %rate_h.1, ...), custom_call_target="tpu_custom_call" | custom-call | tf_op jit(solution)/shard_map/mixer/pallas_call | solution.py:578
  69.9 0.7 store.1

commit v4 on v3

--- a/solution.py
+++ b/solution.py
@@ -102,7 +102,7 @@
     pk_own, aux_own, pk_z, aux_z, pk_y, aux_y,
     wa_in, wb_in, wa_out, wb_out,
     d_send, d_recv, b_send, b_recv,
-    f_own, f_recv, t_own, t_recv, a_own, a_recv, q_own, q_recv,
+    f_own, f_recv, a_own, a_recv, w_re, w_im,
     gat_own, gat_all, mix_own, mix_all,
     go_sa, go_sb, go_ha, go_hb, go_ra, go_rb, go_s2a, go_s2b, go_r2a, go_r2b,
     gi_sa, gi_sb, gi_ha, gi_hb, gi_ra, gi_rb, gi_s2a, gi_s2b, gi_r2a, gi_r2b,
@@ -359,7 +359,6 @@
     u_re[...], u_im[...] = up
     v_re[...], v_im[...] = down
     dec_chunk = factor
-    dec_row = square(dec_chunk, log2(ny))
 
     def total(recv):
         s = recv[0].astype(F32)
@@ -370,26 +369,32 @@
     arrive(DRIVE, "d", d_recv.at[0 : nd - 1])
     x = total(d_recv)
 
-    def carried(recv, n, me, decay, reverse):
-        zero = jnp.zeros((1, lanes), F32)
-        enter, whole, power = (zero, zero), (zero, zero), (zero + 1.0, zero)
-        for i in range(n):
-            j = n - 1 - i if reverse else i
-            piece = (recv[j, 0:1, :], recv[j, 1:2, :])
-            before = j > me if reverse else j < me
-            grown = cmul(enter, decay)
-            enter = (
-                jnp.where(before, grown[0] + piece[0], enter[0]),
-                jnp.where(before, grown[1] + piece[1], enter[1]),
-            )
-            grown = cmul(whole, decay)
-            whole = (grown[0] + piece[0], grown[1] + piece[1])
-            grown = cmul(power, decay)
-            power = (
-                jnp.where(before, grown[0], power[0]),
-                jnp.where(before, grown[1], power[1]),
-            )
-        return enter, whole, power
+    chunks = ny * nz
+
+    def to_all(phase, own, recv, reverse):
+        far = lambda k, n: min(k, n - k)
+        offsets = [(a, b) for a in range(nz) for b in range(ny) if a or b]
+        for a, b in sorted(offsets, key=lambda o: -far(o[0], nz) - far(o[1], ny)):
+            j = peer("z", a) * ny + peer("y", b)
+            ahead = sp - j if reverse else j - sp
+            pltpu.make_async_remote_copy(
+                src_ref=own,
+                dst_ref=recv.at[lax.rem(ahead - 1 + 2 * chunks, chunks)],
+                send_sem=ssem.at[phase],
+                recv_sem=rsem.at[phase],
+                device_id=(j, dp),
+                device_id_type=MESH,
+            ).start()
+        sent.append((phase, "y", recv.at[1:]))
+
+    def entering(recv, reverse):
+        held = iota((chunks, 2, lanes), 0) < (chunks - 1 - sp if reverse else sp)
+        state = jnp.where(held, recv[...], 0.0)
+        by_re = jnp.sum(state * w_re[...], axis=0)
+        by_im = jnp.sum(state * w_im[...], axis=0)
+        if reverse:
+            by_im = -by_im
+        return by_re[0:1] - by_im[1:2], by_re[1:2] + by_im[0:1]
 
     def summed(pair, table_re, table_im, sign):
         tr, ti = table_re[...], sign * table_im[...]
@@ -403,23 +408,23 @@
     push = (dot(x, bre[...]), dot(x, bim[...]))
     final = summed(push, v_re, v_im, 1.0)
     put(f_own, final)
-    send(FWD_Y, "y", lambda k: f_own, lambda k: f_recv.at[y], f_recv.at[0 : ny - 1])
-    put(f_recv.at[y], final)
+    to_all(FWD_Y, f_own, f_recv, False)
     local = scan_rows(push, dec, False)
     gathered(OUT_A2, "z", wa_out)
     gathered(OUT_B2, "y", wb_out)
     project(BACK, cot, wa_out, wb_out, b_send, b_recv)
 
-    arrive(FWD_Y, "y", f_recv.at[0 : ny - 1])
-    enter_y, whole_y, power_y = carried(f_recv, ny, y, dec_chunk, False)
-    put(t_own, whole_y)
-    send(FWD_Z, "z", lambda k: t_own, lambda k: t_recv.at[z], t_recv.at[0 : nz - 1])
-    put(t_recv.at[z], whole_y)
-
-    arrive(FWD_Z, "z", t_recv.at[0 : nz - 1])
-    enter_z, _, _ = carried(t_recv, nz, z, dec_row, False)
-    far = cmul(power_y, enter_z)
-    start = cmul(dec, (enter_y[0] + far[0], enter_y[1] + far[1]))
+    row = iota((chunks, lanes), 0)
+    power, factor = (jnp.ones((chunks, lanes), F32), jnp.zeros((chunks, lanes), F32)), dec_chunk
+    for k in range(log2(chunks)):
+        bit = lax.rem(lax.div(row, 1 << k), 2) == 1
+        more = cmul(power, factor)
+        power = (jnp.where(bit, more[0], power[0]), jnp.where(bit, more[1], power[1]))
+        factor = square(factor, 1)
+    w_re[...] = jnp.broadcast_to(power[0][:, None, :], (chunks, 2, lanes))
+    w_im[...] = jnp.broadcast_to(power[1][:, None, :], (chunks, 2, lanes))
+    arrive(FWD_Y, "y", f_recv.at[1:])
+    start = cmul(dec, entering(f_recv, False))
     add = cmul((u_re[...], u_im[...]), start)
     state_re, state_im = (local[0] + add[0]).astype(BF16), (local[1] + add[1]).astype(BF16)
     mixed = dot(state_re, cre[...], NT) - dot(state_im, cim[...], NT) + gain * x.astype(F32)
@@ -435,19 +440,12 @@
     pulled = (dot(inner_b, cre[...]), -dot(inner_b, cim[...]))
     opening = summed(pulled, u_re, u_im, -1.0)
     put(a_own, opening)
-    send(BWD_Y, "y", lambda k: a_own, lambda k: a_recv.at[y], a_recv.at[0 : ny - 1])
-    put(a_recv.at[y], opening)
+    to_all(BWD_Y, a_own, a_recv, True)
     gat_own[...] = gated
     send(GATED, "d", lambda k: gat_own, lambda k: gat_all.at[dp], gat_all.at[0 : nd - 1])
     gat_all[dp] = gated
     back_dec = conj(dec)
     local = scan_rows(pulled, back_dec, True)
-    arrive(BWD_Y, "y", a_recv.at[0 : ny - 1])
-    enter_y, whole_y, power_y = carried(a_recv, ny, y, conj(dec_chunk), True)
-    put(q_own, whole_y)
-    send(BWD_Z, "z", lambda k: q_own, lambda k: q_recv.at[z], q_recv.at[0 : nz - 1])
-    put(q_recv.at[z], whole_y)
-
     def block_of_grad(b, cols, act, sa, sb):
         part = dot(cols[b], act[...], TN).astype(BF16)
         sa[b] = part[:, 0:half].reshape(ny, per_group, half)
@@ -510,10 +508,8 @@
     hand_on(GO_A1, GO_HA, "z", go_sa, go_ha, go_ra)
     hand_on(GO_B1, GO_HB, "y", go_sb, go_hb, go_rb)
 
-    arrive(BWD_Z, "z", q_recv.at[0 : nz - 1])
-    enter_z, _, _ = carried(q_recv, nz, z, conj(dec_row), True)
-    far = cmul(power_y, enter_z)
-    start = cmul(back_dec, (enter_y[0] + far[0], enter_y[1] + far[1]))
+    arrive(BWD_Y, "y", a_recv.at[1:])
+    start = cmul(back_dec, entering(a_recv, True))
     add = cmul((v_re[...], -v_im[...]), start)
     adj_re, adj_im = (local[0] + add[0]).astype(BF16), (local[1] + add[1]).astype(BF16)
     mix = (dot(adj_re, bre[...], NT) + dot(adj_im, bim[...], NT) + gain * inner).astype(BF16)
@@ -521,22 +517,23 @@
     send(MIX, "d", lambda k: mix_own, lambda k: mix_all.at[dp], mix_all.at[0 : nd - 1], lambda k: mix_sem.at[k])
     mix_all[dp] = mix
 
-    pass_on(GO_A1, GO_HA, "z", go_sa, go_ha, go_ra)
-    pass_on(GO_B1, GO_HB, "y", go_sb, go_hb, go_rb)
     block_of_grad(dp, mix_all, tok, gi_sa, gi_sb)
-    for k in ring_order(nd, False):
+    for i, k in enumerate(ring_order(nd, False)):
         j = peer("d", nd - k)
         copy(MIX, "d", j, mix_own, mix_all.at[j], mix_sem.at[k]).wait_recv()
         block_of_grad(j, mix_all, tok, gi_sa, gi_sb)
+        if i == min(1, nd - 2):
+            pass_on(GO_A1, GO_HA, "z", go_sa, go_ha, go_ra)
+            pass_on(GO_B1, GO_HB, "y", go_sb, go_hb, go_rb)
     hand_on(GI_A1, GI_HA, "z", gi_sa, gi_ha, gi_ra)
     hand_on(GI_B1, GI_HB, "y", gi_sb, gi_hb, gi_rb)
-    second_step(GO_A1, GO_B1, GO_A2, GO_B2, go_ra, go_rb, go_s2a, go_s2b, go_r2a, go_r2b)
     grad = dot(mix_all[0], weights_of(wa_in, wb_in, 0))
     for b in range(1, nd):
         grad = grad + dot(mix_all[b], weights_of(wa_in, wb_in, b))
     o_tok[...] = grad.astype(BF16)
     pass_on(GI_A1, GI_HA, "z", gi_sa, gi_ha, gi_ra)
     pass_on(GI_B1, GI_HB, "y", gi_sb, gi_hb, gi_rb)
+    second_step(GO_A1, GO_B1, GO_A2, GO_B2, go_ra, go_rb, go_s2a, go_s2b, go_r2a, go_r2b)
     second_step(GI_A1, GI_B1, GI_A2, GI_B2, gi_ra, gi_rb, gi_s2a, gi_s2b, gi_r2a, gi_r2b)
     finish(GO_A2, GO_B2, go_r2a, go_r2b, o_out)
     finish(GI_A2, GI_B2, gi_r2a, gi_r2b, o_in)
@@ -593,10 +590,9 @@
             V((nz, ny, c, half), BF16), V((ny, nz, c, half), BF16),
             V((nd, rows, own_ch), BF16), V((nd, rows, own_ch), BF16),
             V((nd, rows, own_ch), BF16), V((nd, rows, own_ch), BF16),
-            V((2, lanes), F32), V((ny, 2, lanes), F32),
-            V((2, lanes), F32), V((nz, 2, lanes), F32),
-            V((2, lanes), F32), V((ny, 2, lanes), F32),
-            V((2, lanes), F32), V((nz, 2, lanes), F32),
+            V((2, lanes), F32), V((ny * nz, 2, lanes), F32),
+            V((2, lanes), F32), V((ny * nz, 2, lanes), F32),
+            V((ny * nz, 2, lanes), F32), V((ny * nz, 2, lanes), F32),
             V((rows, own_ch), BF16), V((nd, rows, own_ch), BF16),
             V((rows, own_ch), BF16), V((nd, rows, own_ch), BF16),
             *relayed, *relayed,

time: 71.5 us -> 68.9 us (0.964); the launches traced: 70.6 us -> 68.7 us
  Pallas kernels: 69.3 us -> 67.4 us
    pallas_call x1, Pallas kernels: 68.6 us -> 66.8 us  [on_device(): pl.pallas_call(functools.partial(kernel, ny, nz, nd), out_shape=(jax.Shap...]
where the time goes in v4:
time: 68.9 us; the launch traced here: 68.7 us
  Pallas kernels  67.4 us (98%)
  between operations  1.29 us (2%)
    pallas_call x1, Pallas kernels, on_device(): pl.pallas_call(functools.partial(kernel, ny, nz, nd), out_shape=(jax.Shap...  66.8 us

profile of v4, /device:TPU:1, one launch (start us, length us, event | category | flops | bytes accessed | tf_op | source)
XLA Modules:
  0.0 68.7 jit_solution(5860359072587829868)
XLA Ops:
  1.3 66.8 %mixer.1 = (bf16[128,256]{1,0:T(8,128)(2,1)S(1)}, f32[16,256]{1,0:T(8,128)S(1)}, f32[16,256]{1,0:T(8,128)S(1)}) custom-call(f32[1]{0:T(128)S(6)} %copy.15.slog, bf16[128,256]{1,0:T(8,128)(2,1)} %tok_h.1, bf16[128,256]{1,0:T(8,128)(2,1)} %cot_h.1, bf16[16,256]{1,0:T(8,128)(2,1)} %win_h.1, bf16[16,256]{1,0:T(8,128)(2,1)} %wout_h.1, f32[1,32]{1,0:T(1,128)} %rate_h.1, ...), custom_call_target="tpu_custom_call" | custom-call | tf_op jit(solution)/shard_map/mixer/pallas_call | solution.py:575
  68.1 0.7 store.1

commit v5 on v4

--- a/solution.py
+++ b/solution.py
@@ -299,33 +299,32 @@
 
     for load in loads[9:]:
         load.wait()
-    for at in range(nz):
-        for part, (a, e) in enumerate(parts(nz)):
-            if at == a:
-                got = wb_in.at[1:, a:e]
-                with jax.named_scope("IN_B%d" % at):
-                    copy(IN_B2, "y", peer("y", 1), got, got, in2_sem.at[1, part]).wait_recv()
-        if at:
-            with jax.named_scope("IN_A%d" % at):
-                copy(IN_A2, "z", peer("z", 1), wa_in.at[at], wa_in.at[at], in2_sem.at[0, at]).wait_recv()
-        b = peer("z", slots(nz)[0][at])
-        d_send[b] = dot(tok[...], weights_at(wa_in, wb_in, at), NT).astype(BF16)
-
-        @pl.when(b != dp)
-        def _():
-            copy(DRIVE, "d", b, d_send.at[b], d_recv.at[dp]).start()
-
-        @pl.when(b == dp)
-        def _():
-            d_recv[dp] = d_send[dp]
+    for part, (a, e) in enumerate(parts(nz)):
+        got = wb_in.at[1:, a:e]
+        copy(IN_B2, "y", peer("y", 1), got, got, in2_sem.at[1, part]).wait_recv()
+        for at in range(max(a, 1), e):
+            copy(IN_A2, "z", peer("z", 1), wa_in.at[at], wa_in.at[at], in2_sem.at[0, at]).wait_recv()
+        targets = [peer("z", slots(nz)[0][at]) for at in range(a, e)]
+        for at, b in zip(range(a, e), targets):
+            d_send[b] = dot(tok[...], weights_at(wa_in, wb_in, at), NT).astype(BF16)
+
+            @pl.when(b != dp)
+            def _():
+                copy(DRIVE, "d", b, d_send.at[b], d_recv.at[dp]).start()
+
+            @pl.when(b == dp)
+            def _():
+                d_recv[dp] = d_send[dp]
+
+        if part == 1:
+            arrive(OUT_A1, "y", wa_out.at[0, 1:])
+            spread(OUT_A2, "z", wa_out, wa_out.at[0, 0:ny], 0, ny)
+            arrive(OUT_B1, "z", wb_out.at[0, 1:])
+            spread(OUT_B2, "y", wb_out, wb_out.at[0, 0:nz], 0, nz)
 
     sent.append((IN_A2, "z", wa_in.at[1:]))
     sent.append((IN_B2, "y", wb_in.at[1:]))
     sent.append((DRIVE, "d", d_recv.at[0 : nd - 1]))
-    arrive(OUT_A1, "y", wa_out.at[0, 1:])
-    spread(OUT_A2, "z", wa_out, wa_out.at[0, 0:ny], 0, ny)
-    arrive(OUT_B1, "z", wb_out.at[0, 1:])
-    spread(OUT_B2, "y", wb_out, wb_out.at[0, 0:nz], 0, nz)
 
     arrive(PK_Y, "y", pk_y.at[0 : ny - 1])
     arrive(AUX_Y, "y", aux_y.at[0 : ny - 1])
@@ -389,7 +388,7 @@
 
     def entering(recv, reverse):
         held = iota((chunks, 2, lanes), 0) < (chunks - 1 - sp if reverse else sp)
-        state = jnp.where(held, recv[...], 0.0)
+        state = jnp.where(held, recv[...].astype(F32), 0.0)
         by_re = jnp.sum(state * w_re[...], axis=0)
         by_im = jnp.sum(state * w_im[...], axis=0)
         if reverse:
@@ -402,8 +401,7 @@
         return jnp.sum(re, axis=0, keepdims=True), jnp.sum(im, axis=0, keepdims=True)
 
     def put(ref, pair):
-        ref[0:1, :] = pair[0]
-        ref[1:2, :] = pair[1]
+        ref[...] = jnp.concatenate(pair, axis=0).astype(ref.dtype)
 
     push = (dot(x, bre[...]), dot(x, bim[...]))
     final = summed(push, v_re, v_im, 1.0)
@@ -518,11 +516,14 @@
     mix_all[dp] = mix
 
     block_of_grad(dp, mix_all, tok, gi_sa, gi_sb)
-    for i, k in enumerate(ring_order(nd, False)):
-        j = peer("d", nd - k)
-        copy(MIX, "d", j, mix_own, mix_all.at[j], mix_sem.at[k]).wait_recv()
-        block_of_grad(j, mix_all, tok, gi_sa, gi_sb)
-        if i == min(1, nd - 2):
+    order = ring_order(nd, False)
+    for batch in (order[0:1], order[1:2], order[2:]):
+        for k in batch:
+            j = peer("d", nd - k)
+            copy(MIX, "d", j, mix_own, mix_all.at[j], mix_sem.at[k]).wait_recv()
+        for k in batch:
+            block_of_grad(peer("d", nd - k), mix_all, tok, gi_sa, gi_sb)
+        if batch == order[1:2]:
             pass_on(GO_A1, GO_HA, "z", go_sa, go_ha, go_ra)
             pass_on(GO_B1, GO_HB, "y", go_sb, go_hb, go_rb)
     hand_on(GI_A1, GI_HA, "z", gi_sa, gi_ha, gi_ra)
@@ -590,8 +591,8 @@
             V((nz, ny, c, half), BF16), V((ny, nz, c, half), BF16),
             V((nd, rows, own_ch), BF16), V((nd, rows, own_ch), BF16),
             V((nd, rows, own_ch), BF16), V((nd, rows, own_ch), BF16),
-            V((2, lanes), F32), V((ny * nz, 2, lanes), F32),
-            V((2, lanes), F32), V((ny * nz, 2, lanes), F32),
+            V((2, lanes), BF16), V((ny * nz, 2, lanes), BF16),
+            V((2, lanes), BF16), V((ny * nz, 2, lanes), BF16),
             V((ny * nz, 2, lanes), F32), V((ny * nz, 2, lanes), F32),
             V((rows, own_ch), BF16), V((nd, rows, own_ch), BF16),
             V((rows, own_ch), BF16), V((nd, rows, own_ch), BF16),

time: 68.9 us -> 68.1 us (0.988)
  Pallas kernels: 67.4 us -> 66.7 us
    pallas_call x1, Pallas kernels: 66.8 us -> 66.1 us  [on_device(): pl.pallas_call(functools.partial(kernel, ny, nz, nd), out_shape=(jax.Shap...]
where the time goes in v5:
time: 68.1 us; the launch traced here: 68 us
  Pallas kernels  66.7 us (98%)
  between operations  1.29 us (2%)
    pallas_call x1, Pallas kernels, on_device(): pl.pallas_call(functools.partial(kernel, ny, nz, nd), out_shape=(jax.Shap...  66.1 us

profile of v5, /device:TPU:1, one launch (start us, length us, event | category | flops | bytes accessed | tf_op | source)
XLA Modules:
  0.0 68.0 jit_solution(13148386000847076617)
XLA Ops:
  1.3 66.1 %mixer.1 = (bf16[128,256]{1,0:T(8,128)(2,1)S(1)}, f32[16,256]{1,0:T(8,128)S(1)}, f32[16,256]{1,0:T(8,128)S(1)}) custom-call(f32[1]{0:T(128)S(6)} %copy.15.slog, bf16[128,256]{1,0:T(8,128)(2,1)} %tok_h.1, bf16[128,256]{1,0:T(8,128)(2,1)} %cot_h.1, bf16[16,256]{1,0:T(8,128)(2,1)} %win_h.1, bf16[16,256]{1,0:T(8,128)(2,1)} %wout_h.1, f32[1,32]{1,0:T(1,128)} %rate_h.1, ...), custom_call_target="tpu_custom_call" | custom-call | tf_op jit(solution)/shard_map/mixer/pallas_call | solution.py:576
  67.4 0.7 store.1

commit v6 on v5

--- a/solution.py
+++ b/solution.py
@@ -523,11 +523,10 @@
             copy(MIX, "d", j, mix_own, mix_all.at[j], mix_sem.at[k]).wait_recv()
         for k in batch:
             block_of_grad(peer("d", nd - k), mix_all, tok, gi_sa, gi_sb)
-        if batch == order[1:2]:
-            pass_on(GO_A1, GO_HA, "z", go_sa, go_ha, go_ra)
-            pass_on(GO_B1, GO_HB, "y", go_sb, go_hb, go_rb)
     hand_on(GI_A1, GI_HA, "z", gi_sa, gi_ha, gi_ra)
     hand_on(GI_B1, GI_HB, "y", gi_sb, gi_hb, gi_rb)
+    pass_on(GO_A1, GO_HA, "z", go_sa, go_ha, go_ra)
+    pass_on(GO_B1, GO_HB, "y", go_sb, go_hb, go_rb)
     grad = dot(mix_all[0], weights_of(wa_in, wb_in, 0))
     for b in range(1, nd):
         grad = grad + dot(mix_all[b], weights_of(wa_in, wb_in, b))

time: 68.1 us -> 67.6 us (level)
  the two profiles are of different devices: /device:TPU:1 before, /device:TPU:8 now
where the time goes in v6:
time: 67.6 us; the launch traced here: 67.5 us
  Pallas kernels  66.2 us (98%)
  between operations  1.29 us (2%)
    pallas_call x1, Pallas kernels, on_device(): pl.pallas_call(functools.partial(kernel, ny, nz, nd), out_shape=(jax.Shap...  65.5 us

profile of v6, /device:TPU:8, one launch (start us, length us, event | category | flops | bytes accessed | tf_op | source)
XLA Modules:
  0.0 67.5 jit_solution(14735147724709491736)
XLA Ops:
  1.3 65.5 %mixer.1 = (bf16[128,256]{1,0:T(8,128)(2,1)S(1)}, f32[16,256]{1,0:T(8,128)S(1)}, f32[16,256]{1,0:T(8,128)S(1)}) custom-call(f32[1]{0:T(128)S(6)} %copy.15.slog, bf16[128,256]{1,0:T(8,128)(2,1)} %tok_h.1, bf16[128,256]{1,0:T(8,128)(2,1)} %cot_h.1, bf16[16,256]{1,0:T(8,128)(2,1)} %win_h.1, bf16[16,256]{1,0:T(8,128)(2,1)} %wout_h.1, f32[1,32]{1,0:T(1,128)} %rate_h.1, ...), custom_call_target="tpu_custom_call" | custom-call | tf_op jit(solution)/shard_map/mixer/pallas_call | solution.py:575
  66.8 0.7 store.1
